TPU v7x, 32 devices: a whole 2x2x4 slice. The times are simulated.
32 devices in a mesh: grp: 2 (over y), fs: 8 (over z, core), tp: 2 (over x).
Axes of the slice: x: 2, y: 2, z: 4, core: 2. Of those that a mesh axis runs over, the one named last changes fastest.
Arguments:
- prompt: bfloat16 [6144, 2048], P(('grp', 'fs')), parts along dimension 0, may hold values from -6 to 6
- routes: int32 [6144, 4], P(('grp', 'fs')), parts along dimension 0, may hold values from 0 to 7, all different within a row; in each aligned block of 384 rows (0 to 383, 384 to 767, ...) at most 240 rows name the same one
- route_weight: float32 [6144, 4], P(('grp', 'fs')), parts along dimension 0, may hold values from 0.2 to 1
- norm_gain: float32 [2048], P('fs'), may hold values from 0.1 to 1.9
- gate_train: float32 [8, 2048, 1024], P(None, 'fs', 'tp'), may hold values from -0.4 to 0.4
- up_train: float32 [8, 2048, 1024], P(None, 'fs', 'tp'), may hold values from -0.4 to 0.4
- down_train: float32 [8, 1024, 2048], P(None, 'fs', 'tp'), may hold values from -0.07 to 0.07
Outputs:
- gate_serve: bfloat16 [16, 2048, 1024], P(('grp', 'fs'), None, 'tp'), parts along dimension 0
- up_serve: bfloat16 [16, 2048, 1024], P(('grp', 'fs'), None, 'tp'), parts along dimension 0
- down_serve: bfloat16 [16, 1024, 2048], P(('grp', 'fs'), 'tp'), parts along dimension 0
- mixed: bfloat16 [6144, 2048], P(('grp', 'fs'), 'tp'), parts along dimension 0
There are 2 independent parts, one for each index of `grp`. A program takes and returns all parts, laid end to end along the dimension named above; an argument that names none is the same for every part. Nothing has to cross between parts.
Inputs may be any that keep to these rules, and one draw needn't show every extreme that they name: `routes`: each row names 4 different experts. Among the rows of one index of fs no expert is named more than 240 times, a bound that some block reaches on some index.
All inputs are finite; a program needn't handle non-finite values.
Results may differ from a plain program's by a relative error of at most 0.012.
Values may be sent and summed in bfloat16 or wider, within the bound.
A program may use at most 128 MiB of HBM per device.

v0:
```python
import functools

import jax
import jax.numpy as jnp
from jax import lax
from jax.experimental import pallas as pl
from jax.experimental.pallas import tpu as pltpu
from jax.sharding import PartitionSpec as P

LIMIT = 7.0
ALPHA = 1.702
EPS = 1e-06
MESH = pl.DeviceIdType.MESH


def exchange(
    sizes,
    scale_in,
    tok_in,
    gate_in,
    up_in,
    down_in,
    scale,
    tok,
    gate,
    up,
    down,
    recv_w,
    send_w,
    recv_t,
    send_up,
    send_dn,
    send_pt,
    recv_s,
    send_s,
    local,
):
    G, F, T = sizes
    g, f, t = lax.axis_index("grp"), lax.axis_index("fs"), lax.axis_index("tp")
    barrier = pltpu.get_barrier_semaphore()
    for axis, here, count in (("fs", f, F), ("grp", g, G), ("tp", t, T)):
        for s in range(1, count):
            pl.semaphore_signal(
                barrier, inc=1, device_id={axis: lax.rem(here + s, count)}, device_id_type=MESH
            )
    pl.semaphore_wait(barrier, F + G + T - 3)

    def remote(src, dst, send, recv, **where):
        return pltpu.make_async_remote_copy(
            src_ref=src, dst_ref=dst, send_sem=send, recv_sem=recv, device_id=where,
            device_id_type=MESH,
        )

    mats = ((gate_in, gate), (up_in, up), (down_in, down))

    def rows_of(m, src, gg, tt):
        block = mats[m][0].shape[1]
        piece = block // G
        start = (tt * F + src) * block + gg * piece
        return mats[m][1].at[pl.ds(pl.multiple_of(start, piece), piece)]

    def sent_piece(m, expert):
        piece = mats[m][0].shape[1] // G
        return mats[m][0].at[expert, pl.ds(pl.multiple_of(g * piece, piece), piece)]

    def wait_piece(m, src, gg, tt):
        ref = rows_of(m, src, gg, tt)
        remote(ref, ref, send_w.at[m], recv_w.at[m, src, gg, tt], fs=lax.rem(f + 1, F)).wait_recv()

    def pass_on(m, src, gg, tt, **where):
        ref = rows_of(m, src, gg, tt)
        remote(ref, ref, send_w.at[m], recv_w.at[m, src, gg, tt], **where).start()

    rows = tok_in.shape[0]

    def block_of(src):
        return tok.at[pl.ds(pl.multiple_of(src * rows, rows), rows)]

    Z = F // 2
    z, core = f // 2, lax.rem(f, 2)
    partner = f + 1 - 2 * core

    own_scale = pltpu.make_async_copy(scale_in.at[f], scale.at[f], local.at[4])
    own_scale.start()

    def scale_copy(to, src):
        return remote(scale_in.at[to], scale.at[src], send_s.at[to], recv_s.at[src], fs=to)

    own = [pltpu.make_async_copy(tok_in, block_of(f), local.at[3])]
    for m in range(3):
        own.append(pltpu.make_async_copy(sent_piece(m, f), rows_of(m, f, g, t), local.at[m]))
    for copy in own:
        copy.start()

    @pl.loop(1, F)
    def _(s):
        scale_copy(lax.rem(f + s, F), f).start()

    for m in range(3):

        @pl.loop(1, F)
        def _(s, m=m):
            to = lax.rem(f + s, F)
            remote(
                sent_piece(m, to), rows_of(m, f, g, t), send_w.at[m], recv_w.at[m, f, g, t], fs=to
            ).start()

    def tok_copy(src_ref, src, kind):
        sems, to = ((send_up, f + 2), (send_dn, f - 2), (send_pt, partner))[kind]
        return remote(src_ref, block_of(src), sems.at[src], recv_t.at[src], fs=to)

    @pl.when(z < Z - 1)
    def _():
        tok_copy(tok_in, f, 0).start()

    @pl.when(z > 0)
    def _():
        tok_copy(tok_in, f, 1).start()

    tok_copy(tok_in, f, 2).start()

    def first(m, src):
        for dg in range(1, G):
            pass_on(m, src, g, t, grp=lax.rem(g + dg, G))
        for dt in range(1, T):
            pass_on(m, src, g, t, tp=lax.rem(t + dt, T))

    def phase1(m):
        own[m + 1].wait()
        first(m, f)

        @pl.loop(1, F)
        def _(s):
            src = lax.rem(f - s + F, F)
            wait_piece(m, src, g, t)
            first(m, src)

    def phase2(m):
        @pl.loop(0, F)
        def _(s):
            src = lax.rem(f - s + F, F)
            even = lax.rem(src, 2) == 0
            for dg in range(1, G):
                gg = lax.rem(g + dg, G)
                wait_piece(m, src, gg, t)

                @pl.when(even)
                def _():
                    for dt in range(1, T):
                        pass_on(m, src, gg, t, tp=lax.rem(t + dt, T))

            for dt in range(1, T):
                tt = lax.rem(t + dt, T)
                wait_piece(m, src, g, tt)

                @pl.when(jnp.logical_not(even))
                def _():
                    for dg in range(1, G):
                        pass_on(m, src, g, tt, grp=lax.rem(g + dg, G))

    def chain(low, high):
        @pl.loop(low, high)
        def _(d):
            @pl.when(z >= d)
            def _():
                src = f - 2 * d
                tok_copy(block_of(src), src, 2).wait_recv()

                @pl.when(z < Z - 1)
                def _():
                    tok_copy(block_of(src), src, 0).start()

                tok_copy(block_of(src), src, 2).start()

            @pl.when(z + d < Z)
            def _():
                src = f + 2 * d
                tok_copy(block_of(src), src, 2).wait_recv()

                @pl.when(z > 0)
                def _():
                    tok_copy(block_of(src), src, 1).start()

                tok_copy(block_of(src), src, 2).start()

    phase1(0)
    phase1(1)
    phase2(0)
    phase1(2)
    chain(1, 2)
    phase2(1)
    chain(2, 3)
    phase2(2)
    chain(3, Z)

    for m in range(3):

        @pl.loop(0, F)
        def _(src, m=m):
            for dg in range(1, G):
                for dt in range(1, T):
                    wait_piece(m, src, lax.rem(g + dg, G), lax.rem(t + dt, T))

        out = mats[m][1]
        sent = out.at[pl.ds(0, out.shape[0] - mats[m][0].shape[1] // G)]
        remote(sent, sent, send_w.at[m], recv_w.at[m, 0, 0, 0], fs=lax.rem(f + 1, F)).wait_send()

    own[0].wait()
    own_scale.wait()

    @pl.loop(1, F)
    def _(s):
        to = lax.rem(f + s, F)
        scale_copy(to, to).wait_recv()
        scale_copy(to, f).wait_send()

    @pl.loop(0, Z)
    def _(zz):
        src = 2 * zz + core
        other = 2 * zz + 1 - core
        tok_copy(block_of(other), other, 2).wait_recv()
        tok_copy(block_of(src), src, 2).wait_send()

        @pl.when(jnp.logical_and(zz <= z, z < Z - 1))
        def _():
            tok_copy(block_of(src), src, 0).wait_send()

        @pl.when(jnp.logical_and(zz >= z, z > 0))
        def _():
            tok_copy(block_of(src), src, 1).wait_send()


def gathered(mesh, scale_in, tok_in, gate_in, up_in, down_in):
    G, F, T = (mesh.shape[name] for name in ("grp", "fs", "tp"))
    full = [
        jax.ShapeDtypeStruct((T * F * w.shape[1], w.shape[2]), w.dtype)
        for w in (gate_in, up_in, down_in)
    ]
    return pl.pallas_call(
        functools.partial(exchange, (G, F, T)),
        out_shape=[jax.ShapeDtypeStruct(scale_in.shape, scale_in.dtype)]
        + [jax.ShapeDtypeStruct((F * tok_in.shape[0], tok_in.shape[1]), tok_in.dtype)]
        + full,
        in_specs=[pl.BlockSpec(memory_space=pl.ANY)] * 5,
        out_specs=[pl.BlockSpec(memory_space=pltpu.VMEM)] * 5,
        scratch_shapes=[
            pltpu.SemaphoreType.DMA((3, F, G, T)),
            pltpu.SemaphoreType.DMA((3,)),
            pltpu.SemaphoreType.DMA((F,)),
            pltpu.SemaphoreType.DMA((F,)),
            pltpu.SemaphoreType.DMA((F,)),
            pltpu.SemaphoreType.DMA((F,)),
            pltpu.SemaphoreType.DMA((F,)),
            pltpu.SemaphoreType.DMA((F,)),
            pltpu.SemaphoreType.DMA((5,)),
        ],
        compiler_params=pltpu.CompilerParams(
            collective_id=0, has_side_effects=True, vmem_limit_bytes=40 * 1024 * 1024
        ),
    )(scale_in, tok_in, gate_in, up_in, down_in)


def shards(mesh, prompt, routes, route_weight, norm_gain, gate_train, up_train, down_train):
    T = mesh.shape["tp"]
    t = lax.axis_index("tp")
    experts = gate_train.shape[0]
    tok_rows, width = prompt.shape
    part = tok_rows // T
    values = lax.dynamic_slice_in_dim(prompt, t * part, part, 0).astype(jnp.float32)
    normed = (values * lax.rsqrt(jnp.mean(values * values, axis=-1, keepdims=True) + EPS)).astype(
        jnp.bfloat16
    )
    lanes = jnp.arange(experts, dtype=jnp.int32)
    routes = lax.dynamic_slice_in_dim(routes, t * part, part, 0)
    route_weight = lax.dynamic_slice_in_dim(route_weight, t * part, part, 0)
    scale = jnp.sum(
        jnp.where(routes[:, :, None] == lanes[None, None, :], route_weight[:, :, None], 0.0), axis=1
    )

    gain = norm_gain[None, :, None]
    scale, tokens, gate, up, down = gathered(
        mesh,
        scale.T.reshape(experts, 1, part),
        normed,
        (gain * gate_train).astype(jnp.bfloat16),
        (gain * up_train).astype(jnp.bfloat16),
        down_train.astype(jnp.bfloat16),
    )
    scale = scale.reshape(-1, 1)
    gate, up, down = (w.reshape(T, w.shape[0] // T, w.shape[1]) for w in (gate, up, down))
    own = gate.shape[2]
    gate_mine = lax.dynamic_slice_in_dim(gate, t, 1, 0)
    up_mine = lax.dynamic_slice_in_dim(up, t, 1, 0)
    down_mine = lax.dynamic_slice_in_dim(down, t * own, own, 1)
    down_mine = down_mine.transpose(1, 0, 2).reshape(1, own, -1)

    hidden = []
    for i in range(T):
        gate_pre = jnp.dot(tokens, gate[i], preferred_element_type=jnp.float32)
        up_pre = jnp.dot(tokens, up[i], preferred_element_type=jnp.float32)
        gate_pre = jnp.minimum(gate_pre, LIMIT)
        up_pre = jnp.clip(up_pre, -LIMIT, LIMIT)
        hidden.append(
            ((up_pre + 1.0) * gate_pre * jax.nn.sigmoid(ALPHA * gate_pre)).astype(jnp.bfloat16)
        )
    hidden = jnp.concatenate(hidden, axis=1)
    weighted = [
        (jnp.dot(hidden, down[i], preferred_element_type=jnp.float32) * scale).astype(jnp.bfloat16)
        for i in range(T)
    ]
    summed = jnp.stack(
        [lax.psum_scatter(w, "fs", scatter_dimension=0, tiled=True) for w in weighted]
    )
    summed, gate_mine, up_mine, down_mine = lax.optimization_barrier(
        (summed, gate_mine, up_mine, down_mine)
    )
    mixed = lax.all_to_all(summed, "tp", split_axis=0, concat_axis=0, tiled=True)
    mixed = mixed.reshape(tok_rows, -1)
    return (gate_mine, up_mine, down_mine, mixed)


def solution(mesh):
    return jax.shard_map(
        functools.partial(shards, mesh),
        mesh=mesh,
        in_specs=(
            P(("grp", "fs"), None),
            P(("grp", "fs"), None),
            P(("grp", "fs"), None),
            P("fs"),
            P(None, "fs", "tp"),
            P(None, "fs", "tp"),
            P(None, "fs", "tp"),
        ),
        out_specs=(
            P(("grp", "fs"), None, "tp"),
            P(("grp", "fs"), None, "tp"),
            P(("grp", "fs"), "tp", None),
            P(("grp", "fs"), "tp"),
        ),
        check_vma=False,
    )
```

profile of v0, /device:TPU:8, one launch (start us, length us, event | category | flops | bytes accessed | tf_op | source)
XLA Modules:
  0.0 288.6 jit_solution(9271367192356261891)
XLA Ops:
  7.2 0.0 copy-start
  7.2 0.0 reduce-scatter.5.cloned.1.call-start
  7.2 0.6 copy-done
  7.9 0.1 constant_dynamic-slice_fusion.2
  7.9 0.8 constant_dynamic-slice_fusion.3
  8.7 0.0 copy-start.4
  8.7 1.5 fusion.14
  10.3 1.3 fusion.15.tok_in
  11.6 0.0 copy-start.3
  11.6 0.0 copy-start.7
  11.6 2.7 convert_element_type.31.down_in
  14.3 0.0 copy-done.4
  14.3 0.7 copy-done.3
  15.1 0.0 copy-done.7
  15.1 1.4 multiply_convert_fusion.2
  16.5 131.5 %shard_map.102 = (f32[8,1,192]{2,1,0:T(1,128)S(1)}, bf16[1536,2048]{1,0:T(8,128)(2,1)}, bf16[4096,512]{1,0:T(8,128)(2,1)S(1)}, bf16[4096,512]{1,0:T(8,128)(2,1)}, bf16[2048,1024]{1,0:T(8,128)(2,1)}) custom-call(f32[8,1,192]{2,1,0:T(1,128)S(1)} %reshape.51.scale_in, bf16[192,2048]{1,0:T(8,128)(2,1)S(1)} %fusion.15.tok_in, ...), custom_call_target="tpu_custom_call" | custom-call | tf_op jit(solution)/shard_map/pallas_call | solution.py:239
  148.0 0.0 copy-start.2
  148.0 0.0 copy-start.8
  148.0 9.5 %convolution_minimum_fusion = f32[1536,512]{0,1:T(8,128)} fusion(bf16[1536,2048]{1,0:T(8,128)(2,1)} %get-tuple-element.13, bf16[4096,512]{1,0:T(8,128)(2,1)S(1)} %get-tuple-element.15), kind=kOutput, calls=%fused_computation.6 | convolution fusion | flops 3222011904 | bytes 11534336 | tf_op jit(solution)/shard_map/dot_general | solution.py:299
  157.5 0.0 copy-done.2
  157.5 0.0 copy-done.8
  157.5 0.0 slice-start
  157.5 5.3 %convolution_minimum_fusion.1 = f32[1536,512]{0,1:T(8,128)} fusion(bf16[1536,2048]{1,0:T(8,128)(2,1)S(1)} %copy-done.8, bf16[4096,512]{1,0:T(8,128)(2,1)S(1)} %get-tuple-element.15), kind=kOutput, calls=%fused_computation.7 | convolution fusion | flops 3222011904 | bytes 11534336 | tf_op jit(solution)/shard_map/dot_general | solution.py:299
  162.8 0.1 mul.80
  162.9 0.0 copy-start.6
  162.9 0.0 slice-start.1
  162.9 0.0 copy-start.9
  162.9 8.7 %fusion.6 = bf16[1536,512]{0,1:T(8,128)(2,1)S(1)} fusion(f32[1536,512]{0,1:T(8,128)} %convolution_minimum_fusion, bf16[1536,2048]{1,0:T(8,128)(2,1)} %get-tuple-element.13, bf16[4096,512]{1,0:T(8,128)(2,1)} %get-tuple-element.14), kind=kOutput, calls=%fused_computation.15 | convolution fusion | flops 3228303360 | bytes 13107200 | tf_op jit(solution)/shard_map/dot_general | solution.py:300
  171.6 0.0 slice-done
  171.6 0.0 copy-done.6
  171.6 0.0 slice-done.1
  171.6 0.0 copy-done.9
  171.6 0.0 copy-start.10
  171.6 0.0 copy-start.5
  171.6 4.7 %fusion.7 = bf16[1536,512]{0,1:T(8,128)(2,1)S(1)} fusion(f32[1536,512]{0,1:T(8,128)S(1)} %copy-done.9, bf16[1536,2048]{1,0:T(8,128)(2,1)S(1)} %bitcast.21, bf16[4096,512]{1,0:T(8,128)(2,1)S(1)} %copy-done.6), kind=kOutput, calls=%fused_computation.16 | convolution fusion | flops 3228303360 | bytes 13107200 | tf_op jit(solution)/shard_map/dot_general | solution.py:300
  176.4 0.0 copy-start.12
  176.4 0.0 copy-done.10
  176.4 1.1 copy-done.12
  177.5 0.0 copy-done.5
  177.5 4.9 %multiply_convert_fusion = bf16[1536,1024]{1,0:T(8,128)(2,1)} fusion(f32[1536]{0:T(1024)S(1)} %mul.80, bf16[2048,1024]{1,0:T(8,128)(2,1)S(1)} %copy-done.5, bf16[1536,512]{0,1:T(8,128)(2,1)S(1)} %fusion.6, bf16[1536,512]{0,1:T(8,128)(2,1)S(1)} %fusion.7), kind=kOutput, calls=%fused_computation | convolution fusion | flops 3230662656 | bytes 8396800 | tf_op jit(solution)/shard_map/dot_general | solution.py:308
  182.4 0.0 copy-start.11
  182.4 0.0 copy-start.13
  182.4 0.0 reduce-scatter.5.cloned.1.call-update
  182.4 0.0 reduce-scatter.3.cloned.1.call-start
  182.5 1.3 copy-done.11
  183.8 0.5 copy-done.13
  184.3 6.5 %multiply_convert_fusion.1 = bf16[1536,1024]{1,0:T(8,128)(2,1)} fusion(f32[1536]{0:T(1024)S(1)} %mul.80, bf16[2048,1024]{1,0:T(8,128)(2,1)} %get-tuple-element.16, bf16[1536,512]{0,1:T(8,128)(2,1)S(1)} %copy-done.11, bf16[1536,512]{0,1:T(8,128)(2,1)S(1)} %copy-done.13), kind=kOutput, calls=%fused_computation.1 | convolution fusion | flops 3230662656 | bytes 8394752 | tf_op jit(solution)/shard_map/dot_general | solution.py:308
  190.8 0.0 reduce-scatter.3.cloned.1.call-update
  190.8 1.8 dynamic-slice_bitcast_fusion
  192.6 2.2 copy.14
  194.7 2.8 reshape.55
  197.5 0.0 copy-start.1
  197.5 4.6 %constant_dynamic-slice_fusion = (bf16[1,2048,512]{2,1,0:T(8,128)(2,1)}, bf16[1,2048,512]{2,1,0:T(8,128)(2,1)}) fusion(bf16[2,2048,512]{2,1,0:T(8,128)(2,1)} %bitcast.16, s32[]{:T(128)S(6)} %select_n.18, bf16[2,2048,512]{2,1,0:T(8,128)(2,1)} %bitcast.13), kind=kLoop, calls=%fused_computation.31 | loop fusion | bytes 8388612 | tf_op jit(solution)/shard_map/dynamic_slice | solution.py:293
  202.1 21.3 %reduce-scatter.5.cloned.1.call-done = bf16[192,1024]{1,0:T(8,128)(2,1)} async-done(((bf16[1536,1024]{1,0:T(8,128)(2,1)}), bf16[192,1024]{1,0:T(8,128)(2,1)}) %reduce-scatter.5.cloned.1.call-update) | async-done | bytes 393232 | tf_op jit(solution)/shard_map/reduce_scatter | solution.py:312
  223.4 42.1 %reduce-scatter.3.cloned.1.call-done = bf16[192,1024]{1,0:T(8,128)(2,1)} async-done(((bf16[1536,1024]{1,0:T(8,128)(2,1)}), bf16[192,1024]{1,0:T(8,128)(2,1)}) %reduce-scatter.3.cloned.1.call-update) | async-done | bytes 393232 | tf_op jit(solution)/shard_map/reduce_scatter | solution.py:312
  265.6 1.2 pad_maximum_fusion.3
  266.8 14.1 %all_to_all.5 = bf16[2,192,1024]{2,1,0:T(8,128)(2,1)S(1)} all-to-all(bf16[2,192,1024]{2,1,0:T(8,128)(2,1)S(1)} %pad_maximum_fusion.3), channel_id=1, replica_groups=mesh['grp'=2,'fs'=8,'tp'=2] {'tp'}, dimensions={0} | all-to-all | bytes 1572864 | tf_op jit(solution)/shard_map/all_to_all | solution.py:317
  280.9 0.9 copy.16
  281.8 0.0 copy-done.1
  (5 shorter events, 0.1 us)
Async XLA Ops:
  7.2 0.7 copy-start
  7.2 216.3 %reduce-scatter.5.cloned.1.call-start = ((), (), s32[]{:S(2)}) async-start(), calls=%async_computation.4 | async-start | bytes 3538944 | tf_op jit(solution)/shard_map/reduce_scatter | solution.py:312
  8.7 5.6 %copy-start.4 = (f32[8,256,512]{2,1,0:T(8,128)S(1)}, f32[8,256,512]{2,1,0:T(8,128)}, u32[]{:S(2)}) copy-start(f32[8,256,512]{2,1,0:T(8,128)} %param.11) | copy-start | bytes 12582916
  11.6 3.5 %copy-start.3 = (f32[8,256,512]{2,1,0:T(8,128)S(1)}, f32[8,256,512]{2,1,0:T(8,128)}, u32[]{:S(2)}) copy-start(f32[8,256,512]{2,1,0:T(8,128)} %param.12) | copy-start | bytes 12582916
  11.6 3.4 %copy-start.7 = (f32[256]{0:T(256)S(1)}, f32[256]{0:T(256)}, u32[]{:S(2)}) copy-start(f32[256]{0:T(256)} %param.10) | copy-start | bytes 3076
  148.0 9.5 %copy-start.2 = (bf16[4096,512]{1,0:T(8,128)(2,1)}, bf16[4096,512]{1,0:T(8,128)(2,1)S(1)}, u32[]{:S(2)}) copy-start(bf16[4096,512]{1,0:T(8,128)(2,1)S(1)} %get-tuple-element.15) | copy-start | bytes 12582916
  148.0 9.5 %copy-start.8 = (bf16[1536,2048]{1,0:T(8,128)(2,1)S(1)}, bf16[1536,2048]{1,0:T(8,128)(2,1)}, u32[]{:S(2)}) copy-start(bf16[1536,2048]{1,0:T(8,128)(2,1)} %get-tuple-element.13) | copy-start | bytes 18874372
  157.5 14.1 %slice-start = ((s8[6291456]{0:T(1024)(128)(4,1)}), s8[2097152]{0:T(1024)(128)(4,1)S(1)}, s32[]{:S(2)}) async-start(s8[6291456]{0:T(1024)(128)(4,1)} %bitcast.20), calls=%async_computation.5 | async-start | bytes 4194304
  162.9 8.7 %copy-start.6 = (bf16[4096,512]{1,0:T(8,128)(2,1)S(1)}, bf16[4096,512]{1,0:T(8,128)(2,1)}, u32[]{:S(2)}) copy-start(bf16[4096,512]{1,0:T(8,128)(2,1)} %get-tuple-element.14) | copy-start | bytes 12582916
  162.9 8.7 %slice-start.1 = ((s8[6291456]{0:T(1024)(128)(4,1)}), s8[4194304]{0:T(1024)(128)(4,1)S(1)}, s32[]{:S(2)}) async-start(s8[6291456]{0:T(1024)(128)(4,1)} %bitcast.20), calls=%async_computation.6 | async-start | bytes 8388608
  162.9 8.7 %copy-start.9 = (f32[1536,512]{0,1:T(8,128)S(1)}, f32[1536,512]{0,1:T(8,128)}, u32[]{:S(2)}) copy-start(f32[1536,512]{0,1:T(8,128)} %convolution_minimum_fusion.1) | copy-start | bytes 9437188
  171.6 4.8 %copy-start.10 = (bf16[1536,512]{0,1:T(8,128)(2,1)}, bf16[1536,512]{0,1:T(8,128)(2,1)S(1)}, u32[]{:S(2)}) copy-start(bf16[1536,512]{0,1:T(8,128)(2,1)S(1)} %fusion.6) | copy-start | bytes 4718596
  171.6 5.9 %copy-start.5 = (bf16[2048,1024]{1,0:T(8,128)(2,1)S(1)}, bf16[2048,1024]{1,0:T(8,128)(2,1)}, u32[]{:S(2)}) copy-start(bf16[2048,1024]{1,0:T(8,128)(2,1)} %get-tuple-element.16) | copy-start | bytes 12582916
  176.4 1.1 copy-start.12
  182.4 1.4 copy-start.11
  182.4 1.9 copy-start.13
  182.4 83.1 %reduce-scatter.3.cloned.1.call-start = ((), (), s32[]{:S(2)}) async-start(), calls=%async_computation.3 | async-start | bytes 3538944 | tf_op jit(solution)/shard_map/reduce_scatter | solution.py:312
  197.5 84.3 %copy-start.1 = (f32[384,4]{0,1:T(4,128)S(1)}, f32[384,4]{0,1:T(4,128)}, u32[]{:S(2)}) copy-start(f32[384,4]{0,1:T(4,128)} %param.9) | copy-start | bytes 18436
Sparse Core Ops, SparseCore 0:
  182.6 40.8 reduce-scatter.4
  225.7 39.7 reduce-scatter.2
where the time goes:
time: 292 us; the launch traced here: 289 us
  Pallas kernels  131 us (45%)
  waiting for transfers between devices  63.5 us (22%)
  matrix products  39.6 us (14%)
  local copies, waits for them, and re-layouts  17.5 us (6%)
  between operations  14.3 us (5%)
  blocking collectives  14.1 us (5%)
  other arithmetic  8.15 us (3%)
    pallas_call x1, Pallas kernels, gathered(): pl.pallas_call(functools.partial(exchange, (G, F, T)), out_shape=[jax.Sha...  131 us
    reduce_scatter x2, waiting for transfers between devices, shards(): lax.psum_scatter(w, 'fs', scatter_dimension=0, tiled=True)  63.5 us
    dot_general x2, matrix products, shards(): gate_pre = jnp.dot(tokens, gate[i], preferred_element_type=jnp.float32)  14.8 us
    all_to_all x1, blocking collectives, shards(): lax.all_to_all(summed, 'tp', split_axis=0, concat_axis=0, tiled=True)  14.1 us
    dot_general x2, matrix products, shards(): up_pre = jnp.dot(tokens, up[i], preferred_element_type=jnp.float32)  13.4 us
    dot_general x2, matrix products, shards(): jnp.dot(hidden, down[i], preferred_element_type=jnp.float32) * scale  11.4 us
  transfers between devices with their start and end apart: 2, of which 2 were waited for; matrix products, arithmetic and copies ran while one was open for 6% of the time, Pallas kernels for 0%

commit v1 on v0

--- a/solution.py
+++ b/solution.py
@@ -260,6 +260,219 @@
     )(scale_in, tok_in, gate_in, up_in, down_in)
 
 
+def chunk_rows(rows):
+    return 48 if rows % 48 == 0 else rows
+
+
+def combine(
+    sizes,
+    hidden,
+    down,
+    scale,
+    out,
+    comb,
+    got,
+    up_in,
+    dn_in,
+    pair_s,
+    pair_r,
+    up_s,
+    up_r,
+    dn_s,
+    dn_r,
+    x_s,
+    x_r,
+):
+    G, F, T = sizes
+    f, t = lax.axis_index("fs"), lax.axis_index("tp")
+    Z = F // 2
+    z, core = f // 2, lax.rem(f, 2)
+    partner = f + 1 - 2 * core
+    lower, upper = z > 0, z < Z - 1
+    part, width = got.shape[1], got.shape[2]
+    own = width // T
+    rows = chunk_rows(part)
+    chunks = part // rows
+    inner = hidden.shape[1]
+    tile = min(512, own)
+
+    barrier = pltpu.get_barrier_semaphore()
+
+    def greet(**where):
+        pl.semaphore_signal(barrier, inc=1, device_id=where, device_id_type=MESH)
+
+    greet(fs=partner)
+    for dt in range(1, T):
+        greet(tp=lax.rem(t + dt, T))
+    pl.when(lower)(lambda: greet(fs=f - 2))
+    pl.when(upper)(lambda: greet(fs=f + 2))
+    pl.semaphore_wait(barrier, T + lower.astype(jnp.int32) + upper.astype(jnp.int32))
+
+    def remote(src, dst, send, recv, **where):
+        return pltpu.make_async_remote_copy(
+            src_ref=src, dst_ref=dst, send_sem=send, recv_sem=recv, device_id=where,
+            device_id_type=MESH,
+        )
+
+    def strip(q):
+        return pl.ds(pl.multiple_of(q * rows, rows), rows)
+
+    def pair_copy(d):
+        return remote(comb.at[d, 1 - core], got.at[d], pair_s.at[d], pair_r.at[d], fs=partner)
+
+    def up_copy(d, q):
+        return remote(
+            comb.at[d, core, strip(q)], up_in.at[d, strip(q)], up_s.at[d, q], up_r.at[d, q],
+            fs=f + 2,
+        )
+
+    def dn_copy(d, q):
+        return remote(
+            comb.at[d, core, strip(q)], dn_in.at[d, strip(q)], dn_s.at[d, q], dn_r.at[d, q],
+            fs=f - 2,
+        )
+
+    def x_copy(q, tt, src):
+        start = pl.multiple_of(src * part + q * rows, rows)
+        return remote(
+            comb.at[z, core, strip(q), pl.ds(pl.multiple_of(tt * own, own), own)],
+            out.at[pl.ds(start, rows)], x_s.at[q, tt], x_r.at[q, src], tp=tt,
+        )
+
+    def dest_of(k):
+        half = k // 2
+        d = jnp.where(lax.rem(k, 2) == 0, Z - 1 - half, half)
+        return jnp.where(2 * z < Z, d, Z - 1 - d)
+
+    def add(d, q, extra):
+        here = comb[d, core, strip(q)].astype(jnp.float32)
+        comb[d, core, strip(q)] = (here + extra[d, strip(q)].astype(jnp.float32)).astype(comb.dtype)
+
+    def compute(d):
+        tokens = pl.ds(pl.multiple_of(d * 2 * part, 2 * part), 2 * part)
+
+        @pl.loop(0, width // tile)
+        def _(i):
+            tt, col = i // (own // tile), lax.rem(i, own // tile) * tile
+            weights = down[
+                pl.ds(pl.multiple_of(tt * inner, inner), inner),
+                pl.ds(pl.multiple_of(col, tile), tile),
+            ]
+            value = jnp.dot(hidden[tokens], weights, preferred_element_type=jnp.float32)
+            value = (value * scale[tokens]).astype(comb.dtype)
+            comb[d, :, :, pl.ds(pl.multiple_of(i * tile, tile), tile)] = value.reshape(
+                2, part, tile
+            )
+
+        pair_copy(d).start()
+
+    def paired(d):
+        pair_copy(d).wait_recv()
+
+        @pl.loop(0, chunks)
+        def _(q):
+            add(d, q, got)
+
+            @pl.when(jnp.logical_and(z == 0, d > z))
+            def _():
+                up_copy(d, q).start()
+
+            @pl.when(jnp.logical_and(z == Z - 1, d < z))
+            def _():
+                dn_copy(d, q).start()
+
+    compute(dest_of(0))
+
+    @pl.loop(1, Z)
+    def _(k):
+        compute(dest_of(k))
+        paired(dest_of(k - 1))
+
+    paired(dest_of(Z - 1))
+
+    ups, downs = 2 * z, 2 * (Z - 1 - z)
+    last = jnp.maximum(
+        jnp.where(lower, (Z - 1 - z) * chunks + ups, 0), jnp.where(upper, z * chunks + downs, 0)
+    )
+
+    @pl.loop(0, Z * chunks + 2 * Z)
+    def _(step):
+        u, v, w = step - ups, step - downs, step - last
+        uq, vq = lax.rem(jnp.maximum(u, 0), chunks), lax.rem(jnp.maximum(v, 0), chunks)
+        high, low = Z - 1 - jnp.maximum(u, 0) // chunks, jnp.maximum(v, 0) // chunks
+
+        @pl.when(jnp.logical_and(jnp.logical_and(lower, u >= 0), high >= z))
+        def _():
+            up_copy(high, uq).wait_recv()
+            add(high, uq, up_in)
+
+            @pl.when(high > z)
+            def _():
+                up_copy(high, uq).start()
+
+        @pl.when(jnp.logical_and(jnp.logical_and(upper, v >= 0), low <= z))
+        def _():
+            dn_copy(low, vq).wait_recv()
+            add(low, vq, dn_in)
+
+            @pl.when(low < z)
+            def _():
+                dn_copy(low, vq).start()
+
+        @pl.when(jnp.logical_and(w >= 0, w < chunks))
+        def _():
+            for dt in range(1, T):
+                x_copy(w, lax.rem(t + dt, T), t).start()
+            start = pl.multiple_of(t * part + w * rows, rows)
+            out[pl.ds(start, rows)] = comb[
+                z, core, strip(w), pl.ds(pl.multiple_of(t * own, own), own)
+            ]
+
+    @pl.loop(0, Z)
+    def _(d):
+        pair_copy(d).wait_send()
+
+        @pl.loop(0, chunks)
+        def _(q):
+            @pl.when(jnp.logical_and(upper, d > z))
+            def _():
+                up_copy(d, q).wait_send()
+
+            @pl.when(jnp.logical_and(lower, d < z))
+            def _():
+                dn_copy(d, q).wait_send()
+
+    @pl.loop(0, chunks)
+    def _(q):
+        for dt in range(1, T):
+            tt = lax.rem(t + dt, T)
+            x_copy(q, tt, t).wait_send()
+            x_copy(q, tt, tt).wait_recv()
+
+
+def combined(mesh, hidden, down, scale):
+    G, F, T = (mesh.shape[name] for name in ("grp", "fs", "tp"))
+    Z, part, width = F // 2, hidden.shape[0] // F, down.shape[1] * T
+    chunks = part // chunk_rows(part)
+    block = pltpu.VMEM((Z, part, width), hidden.dtype)
+    pair, flow, cross = (
+        pltpu.SemaphoreType.DMA((Z,)),
+        pltpu.SemaphoreType.DMA((Z, chunks)),
+        pltpu.SemaphoreType.DMA((chunks, T)),
+    )
+    return pl.pallas_call(
+        functools.partial(combine, (G, F, T)),
+        out_shape=jax.ShapeDtypeStruct((T * part, width // T), hidden.dtype),
+        in_specs=[pl.BlockSpec(memory_space=pltpu.VMEM)] * 3,
+        out_specs=pl.BlockSpec(memory_space=pltpu.VMEM),
+        scratch_shapes=[pltpu.VMEM((Z, 2, part, width), hidden.dtype), block, block, block]
+        + [pair, pair, flow, flow, flow, flow, cross, cross],
+        compiler_params=pltpu.CompilerParams(
+            collective_id=1, has_side_effects=True, vmem_limit_bytes=60 * 1024 * 1024
+        ),
+    )(hidden, down, scale)
+
+
 def shards(mesh, prompt, routes, route_weight, norm_gain, gate_train, up_train, down_train):
     T = mesh.shape["tp"]
     t = lax.axis_index("tp")
@@ -304,18 +517,7 @@
             ((up_pre + 1.0) * gate_pre * jax.nn.sigmoid(ALPHA * gate_pre)).astype(jnp.bfloat16)
         )
     hidden = jnp.concatenate(hidden, axis=1)
-    weighted = [
-        (jnp.dot(hidden, down[i], preferred_element_type=jnp.float32) * scale).astype(jnp.bfloat16)
-        for i in range(T)
-    ]
-    summed = jnp.stack(
-        [lax.psum_scatter(w, "fs", scatter_dimension=0, tiled=True) for w in weighted]
-    )
-    summed, gate_mine, up_mine, down_mine = lax.optimization_barrier(
-        (summed, gate_mine, up_mine, down_mine)
-    )
-    mixed = lax.all_to_all(summed, "tp", split_axis=0, concat_axis=0, tiled=True)
-    mixed = mixed.reshape(tok_rows, -1)
+    mixed = combined(mesh, hidden, down.reshape(-1, down.shape[2]), scale)
     return (gate_mine, up_mine, down_mine, mixed)
 
 

time: 292 us -> 248 us (0.85)
  Pallas kernels: 131 us -> 201 us
  waiting for transfers between devices: 63.5 us -> 0 us
  matrix products: 39.6 us -> 19.3 us
  blocking collectives: 14.1 us -> 0 us
  between operations: 14.3 us -> 0.8 us
    pallas_call x0 -> x1, Pallas kernels: none -> 69.3 us  [combined(): pl.pallas_call(functools.partial(combine, (G, F, T)), out_shape=jax.Shape...]
    reduce_scatter x2 -> x0, waiting for transfers between devices: 63.5 us -> none  [shards(): lax.psum_scatter(w, 'fs', scatter_dimension=0, tiled=True)]
    all_to_all x1 -> x0, blocking collectives: 14.1 us -> none  [shards(): lax.all_to_all(summed, 'tp', split_axis=0, concat_axis=0, tiled=True)]
    dot_general x2 -> x0, matrix products: 11.4 us -> none  [shards(): jnp.dot(hidden, down[i], preferred_element_type=jnp.float32) * scale]
    dot_general x2, matrix products: 13.4 us -> 8.61 us  [shards(): up_pre = jnp.dot(tokens, up[i], preferred_element_type=jnp.float32)]
    unnamed x33 -> x13, local copies, waits for them, and re-layouts: 5.25 us -> 1.07 us
    dot_general x2, matrix products: 14.8 us -> 10.7 us  [shards(): gate_pre = jnp.dot(tokens, gate[i], preferred_element_type=jnp.float32)]
    convert_element_type x1, other arithmetic: 1.39 us -> 4.96 us  [shards(): (gain * up_train).astype(jnp.bfloat16)]
  transfers between devices with their start and end apart: 2 -> 0, of which waited for: 2 -> 0; matrix products, arithmetic and copies ran while one was open for 6% -> 0% of each run, Pallas kernels for 0% -> 0%
where the time goes in v1:
time: 248 us; the launch traced here: 246 us
  Pallas kernels  201 us (81%)
  matrix products  19.3 us (8%)
  local copies, waits for them, and re-layouts  14.7 us (6%)
  other arithmetic  10.1 us (4%)
    pallas_call x1, Pallas kernels, gathered(): pl.pallas_call(functools.partial(exchange, (G, F, T)), out_shape=[jax.Sha...  131 us
    pallas_call x1, Pallas kernels, combined(): pl.pallas_call(functools.partial(combine, (G, F, T)), out_shape=jax.Shape...  69.3 us
    dot_general x2, matrix products, shards(): gate_pre = jnp.dot(tokens, gate[i], preferred_element_type=jnp.float32)  10.7 us
    dot_general x2, matrix products, shards(): up_pre = jnp.dot(tokens, up[i], preferred_element_type=jnp.float32)  8.61 us

profile of v1, /device:TPU:8, one launch (start us, length us, event | category | flops | bytes accessed | tf_op | source)
XLA Modules:
  0.0 245.6 jit_solution(13314288919397394535)
XLA Ops:
  0.6 0.0 copy-start
  0.7 1.4 fusion.12
  2.0 1.3 fusion.13.tok_in
  3.4 0.0 copy-done
  3.4 0.1 constant_dynamic-slice_fusion.2
  3.5 0.8 constant_dynamic-slice_fusion.3
  4.3 0.0 copy-start.2
  4.3 5.0 %multiply_convert_fusion = (bf16[8,256,512]{2,1,0:T(8,128)(2,1)S(1)}, bf16[8,256,512]{2,1,0:T(8,128)(2,1)S(1)}) fusion(f32[8,256,512]{2,1,0:T(8,128)} %param.12, f32[256]{0:T(256)} %param.10, f32[8,256,512]{2,1,0:T(8,128)} %param.11), kind=kLoop, calls=%fused_computation | loop fusion | flops 4194304 | bytes 12583936 | tf_op jit(solution)/shard_map/convert_element_type | solution.py:499
  9.2 0.0 copy-done.2
  9.2 0.3 convert_element_type.25.down_in
  9.6 131.3 %shard_map.102 = (f32[8,1,192]{2,1,0:T(1,128)S(1)}, bf16[1536,2048]{1,0:T(8,128)(2,1)}, bf16[4096,512]{1,0:T(8,128)(2,1)S(1)}, bf16[4096,512]{1,0:T(8,128)(2,1)}, bf16[2048,1024]{1,0:T(8,128)(2,1)}) custom-call(f32[8,1,192]{2,1,0:T(1,128)S(1)} %reshape.45.scale_in, bf16[192,2048]{1,0:T(8,128)(2,1)S(1)} %fusion.13.tok_in, ...), custom_call_target="tpu_custom_call" | custom-call | tf_op jit(solution)/shard_map/pallas_call | solution.py:239
  140.9 0.0 copy-start.1
  140.9 0.0 copy-start.4
  140.9 0.0 copy-start.5
  140.9 7.2 %convolution_minimum_fusion.1 = f32[1536,512]{1,0:T(8,128)S(1)} fusion(bf16[1536,2048]{1,0:T(8,128)(2,1)} %get-tuple-element.12, bf16[4096,512]{1,0:T(8,128)(2,1)S(1)} %get-tuple-element.9), kind=kOutput, calls=%fused_computation.5 | convolution fusion | flops 3222011904 | bytes 11534336 | tf_op jit(solution)/shard_map/dot_general | solution.py:512
  148.1 0.0 copy-done.4
  148.1 0.2 copy-done.5
  148.3 4.3 %fusion.7 = bf16[1536,512]{1,0:T(8,128)(2,1)S(1)} fusion(f32[1536,512]{1,0:T(8,128)S(1)} %convolution_minimum_fusion.1, bf16[1536,2048]{1,0:T(8,128)(2,1)S(1)} %copy-done.5, bf16[4096,512]{1,0:T(8,128)(2,1)S(1)} %copy-done.4), kind=kOutput, calls=%fused_computation.14 | convolution fusion | flops 3228303360 | bytes 13107200 | tf_op jit(solution)/shard_map/dot_general | solution.py:513
  152.6 0.0 copy-done.1
  152.6 3.5 %convolution_minimum_fusion = f32[1536,512]{1,0:T(8,128)S(1)} fusion(bf16[1536,2048]{1,0:T(8,128)(2,1)S(1)} %copy-done.5, bf16[4096,512]{1,0:T(8,128)(2,1)S(1)} %get-tuple-element.9), kind=kOutput, calls=%fused_computation.4 | convolution fusion | flops 3222011904 | bytes 11534336 | tf_op jit(solution)/shard_map/dot_general | solution.py:512
  156.2 4.3 %fusion.6 = bf16[1536,512]{1,0:T(8,128)(2,1)S(1)} fusion(f32[1536,512]{1,0:T(8,128)S(1)} %convolution_minimum_fusion, bf16[1536,2048]{1,0:T(8,128)(2,1)S(1)} %copy-done.5, bf16[4096,512]{1,0:T(8,128)(2,1)S(1)} %copy-done.4), kind=kOutput, calls=%fused_computation.13 | convolution fusion | flops 3228303360 | bytes 13107200 | tf_op jit(solution)/shard_map/dot_general | solution.py:513
  160.5 2.1 pad_maximum_fusion.hidden
  162.6 1.5 reshape.51.scale
  164.0 69.3 %shard_map.103 = bf16[384,1024]{1,0:T(8,128)(2,1)} custom-call(bf16[1536,1024]{1,0:T(8,128)(2,1)} %pad_maximum_fusion.hidden, bf16[2048,1024]{1,0:T(8,128)(2,1)} %get-tuple-element.11.down, f32[1536,1]{1,0:T(8,128)} %reshape.51.scale), custom_call_target="tpu_custom_call" | custom-call | tf_op jit(solution)/shard_map/pallas_call | solution.py:463
  233.4 1.8 dynamic-slice_bitcast_fusion
  235.2 2.2 copy.26
  237.3 2.8 %reshape.49 = bf16[1,512,2048]{2,1,0:T(8,128)(2,1)} reshape(bf16[512,2,1024]{2,1,0:T(2,128)(2,1)S(1)} %copy.26) | data formatting | bytes 4194304 | tf_op jit(solution)/shard_map/reshape | solution.py:508
  240.1 0.0 copy-start.3
  240.1 4.6 %constant_dynamic-slice_fusion = (bf16[1,2048,512]{2,1,0:T(8,128)(2,1)}, bf16[1,2048,512]{2,1,0:T(8,128)(2,1)}) fusion(bf16[2,2048,512]{2,1,0:T(8,128)(2,1)} %bitcast.12, s32[]{:T(128)S(6)} %select_n.18, bf16[2,2048,512]{2,1,0:T(8,128)(2,1)} %bitcast.10), kind=kLoop, calls=%fused_computation.26 | loop fusion | bytes 8388612 | tf_op jit(solution)/shard_map/dynamic_slice | solution.py:506
  244.7 0.0 copy-done.3
  244.7 0.9 copy.37
  (4 shorter events, 0.1 us)
Async XLA Ops:
  0.6 2.7 %copy-start = (f32[384,4]{0,1:T(4,128)S(1)}, f32[384,4]{0,1:T(4,128)}, u32[]{:S(2)}) copy-start(f32[384,4]{0,1:T(4,128)} %param.9) | copy-start | bytes 18436
  4.3 5.0 %copy-start.2 = (f32[8,128,1024]{2,1,0:T(8,128)S(1)}, f32[8,128,1024]{2,1,0:T(8,128)}, u32[]{:S(2)}) copy-start(f32[8,128,1024]{2,1,0:T(8,128)} %param.13) | copy-start | bytes 12582916
  140.9 11.7 %copy-start.1 = (bf16[4096,512]{1,0:T(8,128)(2,1)}, bf16[4096,512]{1,0:T(8,128)(2,1)S(1)}, u32[]{:S(2)}) copy-start(bf16[4096,512]{1,0:T(8,128)(2,1)S(1)} %get-tuple-element.9) | copy-start | bytes 12582916
  140.9 7.2 %copy-start.4 = (bf16[4096,512]{1,0:T(8,128)(2,1)S(1)}, bf16[4096,512]{1,0:T(8,128)(2,1)}, u32[]{:S(2)}) copy-start(bf16[4096,512]{1,0:T(8,128)(2,1)} %get-tuple-element.10) | copy-start | bytes 12582916
  140.9 7.4 %copy-start.5 = (bf16[1536,2048]{1,0:T(8,128)(2,1)S(1)}, bf16[1536,2048]{1,0:T(8,128)(2,1)}, u32[]{:S(2)}) copy-start(bf16[1536,2048]{1,0:T(8,128)(2,1)} %get-tuple-element.12) | copy-start | bytes 18874372
  240.1 4.6 %copy-start.3 = (bf16[384,1024]{1,0:T(8,128)(2,1)S(1)}, bf16[384,1024]{1,0:T(8,128)(2,1)}, u32[]{:S(2)}) copy-start(bf16[384,1024]{1,0:T(8,128)(2,1)} %shard_map.103) | copy-start | bytes 2359300

commit v2 on v1

v2 whole, which is shorter than its diff:
```python
import functools

import jax
import jax.numpy as jnp
from jax import lax
from jax.experimental import pallas as pl
from jax.experimental.pallas import tpu as pltpu
from jax.sharding import PartitionSpec as P

LIMIT = 7.0
ALPHA = 1.702
EPS = 1e-06
MESH = pl.DeviceIdType.MESH


def chunk_rows(rows):
    return 48 if rows % 48 == 0 else rows


def layer(
    sizes,
    scale_in,
    tok_in,
    gate_in,
    up_in,
    down_in,
    gate,
    up,
    down,
    out,
    tok,
    hidden,
    comb,
    got,
    above,
    scale,
    weight,
    recv_w,
    send_w,
    recv_t,
    send_up,
    send_dn,
    send_pt,
    recv_s,
    send_s,
    local,
    pair_s,
    pair_r,
    up_s,
    up_r,
    dn_s,
    dn_r,
    x_s,
    x_r,
):
    G, F, T = sizes
    g, f, t = lax.axis_index("grp"), lax.axis_index("fs"), lax.axis_index("tp")
    Z = F // 2
    z, core = f // 2, lax.rem(f, 2)
    partner = f + 1 - 2 * core
    lower, upper = z > 0, z < Z - 1
    part, width = got.shape[1], got.shape[2]
    own = width // T
    rows = chunk_rows(part)
    chunks = part // rows
    inner = hidden.shape[1]
    tile = min(512, own)
    cols = gate.shape[1]
    strips = min(256, cols)
    tiles = inner // strips
    far = F - 2
    lag = far // 2

    barrier = pltpu.get_barrier_semaphore()
    for axis, here, count in (("fs", f, F), ("grp", g, G), ("tp", t, T)):
        for s in range(1, count):
            pl.semaphore_signal(
                barrier, inc=1, device_id={axis: lax.rem(here + s, count)}, device_id_type=MESH
            )
    pl.semaphore_wait(barrier, F + G + T - 3)

    def remote(src, dst, send, recv, **where):
        return pltpu.make_async_remote_copy(
            src_ref=src, dst_ref=dst, send_sem=send, recv_sem=recv, device_id=where,
            device_id_type=MESH,
        )

    mats = ((gate_in, gate), (up_in, up), (down_in, down))

    def block_rows(m, src, tt):
        block = mats[m][0].shape[1]
        return mats[m][1].at[pl.ds(pl.multiple_of((tt * F + src) * block, block), block)]

    def piece_rows(m, src, gg, tt):
        block = mats[m][0].shape[1]
        piece = block // G
        start = (tt * F + src) * block + gg * piece
        return mats[m][1].at[pl.ds(pl.multiple_of(start, piece), piece)]

    def sent_piece(m, expert):
        piece = mats[m][0].shape[1] // G
        return mats[m][0].at[expert, pl.ds(pl.multiple_of(g * piece, piece), piece)]

    def wait_piece(m, src, gg, tt):
        ref = piece_rows(m, src, gg, tt)
        remote(ref, ref, send_w.at[m], recv_w.at[m, src, gg, tt], fs=partner).wait_recv()

    def pass_piece(m, src, gg, tt, **where):
        ref = piece_rows(m, src, gg, tt)
        remote(ref, ref, send_w.at[m], recv_w.at[m, src, gg, tt], **where).start()

    def wait_block(m, src, tt):
        ref = block_rows(m, src, tt)
        remote(ref, ref, send_w.at[m], recv_w.at[m, src, 0, tt], fs=partner).wait_recv()

    def near_blocks(m, src_ref, src):
        for dt in range(1, T):
            remote(
                src_ref, block_rows(m, src, t), send_w.at[m], recv_w.at[m, src, 0, t],
                tp=lax.rem(t + dt, T),
            ).start()

    def far_source(r):
        return lax.rem(f - (r + 1 + core) + F, F)

    def own_block(m):
        return pltpu.make_async_copy(mats[m][0].at[f], block_rows(m, f, t), local.at[m])

    def token_block(src):
        return tok.at[pl.ds(pl.multiple_of(src * part, part), part)]

    def token_rows(src, q):
        return tok.at[pl.ds(pl.multiple_of(src * part + q * rows, rows), rows)]

    own_tokens = pltpu.make_async_copy(tok_in, token_block(f), local.at[3])
    own_scale = pltpu.make_async_copy(scale_in.at[f], scale.at[f], local.at[4])

    def scale_copy(to, src):
        return remote(scale_in.at[to], scale.at[src], send_s.at[to], recv_s.at[src], fs=to)

    def token_copy(src_ref, src, q, kind):
        sems, to = ((send_up, f + 2), (send_dn, f - 2), (send_pt, partner))[kind]
        return remote(src_ref, token_rows(src, q), sems.at[src, q], recv_t.at[src, q], fs=to)

    own_scale.start()
    own_tokens.start()
    for m in range(3):
        own_block(m).start()
        remote(
            mats[m][0].at[partner], block_rows(m, f, t), send_w.at[m], recv_w.at[m, f, 0, t],
            fs=partner,
        ).start()

    @pl.loop(1, F)
    def _(s):
        scale_copy(lax.rem(f + s, F), f).start()

    near_blocks(0, mats[0][0].at[f], f)
    for m in range(3):

        @pl.loop(0, far)
        def _(r, m=m):
            to = lax.rem(f + r + 2 - core, F)
            remote(
                sent_piece(m, to), piece_rows(m, f, g, t), send_w.at[m], recv_w.at[m, f, g, t],
                fs=to,
            ).start()

    @pl.loop(0, chunks)
    def _(q):
        source = tok_in.at[pl.ds(pl.multiple_of(q * rows, rows), rows)]

        @pl.when(upper)
        def _():
            token_copy(source, f, q, 0).start()

        @pl.when(lower)
        def _():
            token_copy(source, f, q, 1).start()

        token_copy(source, f, q, 2).start()

    def first(m, r):
        src = far_source(r)
        wait_piece(m, src, g, t)
        for dg in range(1, G):
            pass_piece(m, src, g, t, grp=lax.rem(g + dg, G))
        for dt in range(1, T):
            pass_piece(m, src, g, t, tp=lax.rem(t + dt, T))

    def second(m, r):
        src = far_source(r)
        across = lax.rem(r, 6) == 0
        for dg in range(1, G):
            gg = lax.rem(g + dg, G)
            wait_piece(m, src, gg, t)

            @pl.when(across)
            def _():
                for dt in range(1, T):
                    pass_piece(m, src, gg, t, tp=lax.rem(t + dt, T))

        for dt in range(1, T):
            tt = lax.rem(t + dt, T)
            wait_piece(m, src, g, tt)

            @pl.when(jnp.logical_not(across))
            def _():
                for dg in range(1, G):
                    pass_piece(m, src, g, tt, grp=lax.rem(g + dg, G))

    def settle(m):
        own_block(m).wait()

        @pl.loop(0, far)
        def _(r):
            for dg in range(1, G):
                for dt in range(1, T):
                    wait_piece(m, far_source(r), lax.rem(g + dg, G), lax.rem(t + dt, T))

        for src in (f, partner):
            for dt in range(1, T):
                wait_block(m, src, lax.rem(t + dt, T))

    for m in range(3):
        if m > 0:
            near_blocks(m, mats[m][0].at[f], f)
        wait_block(m, partner, t)
        near_blocks(m, block_rows(m, partner, t), partner)

        @pl.loop(0, far)
        def _(r, m=m):
            first(m, r)

            @pl.when(r >= lag)
            def _():
                second(m, r - lag)

            if m > 0:

                @pl.when(r < lag)
                def _():
                    second(m - 1, far - lag + r)

    def chain(d, q):
        @pl.when(z >= d)
        def _():
            src = f - 2 * d
            token_copy(token_rows(src, q), src, q, 2).wait_recv()

            @pl.when(upper)
            def _():
                token_copy(token_rows(src, q), src, q, 0).start()

            token_copy(token_rows(src, q), src, q, 2).start()

        @pl.when(z + d < Z)
        def _():
            src = f + 2 * d
            token_copy(token_rows(src, q), src, q, 2).wait_recv()

            @pl.when(lower)
            def _():
                token_copy(token_rows(src, q), src, q, 1).start()

            token_copy(token_rows(src, q), src, q, 2).start()

    def tokens_of(d):
        return pl.ds(pl.multiple_of(d * 2 * part, 2 * part), 2 * part)

    def partner_tokens(d):
        src = 2 * d + 1 - core

        @pl.loop(0, chunks)
        def _(q):
            token_copy(token_rows(src, q), src, q, 2).wait_recv()

    def hidden_tile(d, i):
        per = cols // strips
        tt, col = i // per, lax.rem(i, per) * strips
        where = (
            pl.ds(pl.multiple_of(tt * width, width), width),
            pl.ds(pl.multiple_of(col, strips), strips),
        )
        held = tok[tokens_of(d)]
        gate_pre = jnp.dot(held, gate[where], preferred_element_type=jnp.float32)
        up_pre = jnp.dot(held, up[where], preferred_element_type=jnp.float32)
        gate_pre = jnp.minimum(gate_pre, LIMIT)
        up_pre = jnp.clip(up_pre, -LIMIT, LIMIT)
        value = (up_pre + 1.0) * gate_pre * jax.nn.sigmoid(ALPHA * gate_pre)
        hidden[tokens_of(d), pl.ds(pl.multiple_of(i * strips, strips), strips)] = value.astype(
            hidden.dtype
        )

    own_tokens.wait()
    settle(0)
    settle(1)

    @pl.loop(0, Z)
    def _(d):
        low, high = z - d, z + d
        pl.when(low >= 0)(lambda: partner_tokens(low))
        pl.when(jnp.logical_and(d > 0, high < Z))(lambda: partner_tokens(high))

        @pl.loop(0, chunks)
        def _(q):
            pl.when(d + 1 < Z)(lambda: chain(d + 1, q))

            @pl.when(d == 0)
            def _():
                @pl.loop(far - lag + q * lag // chunks, far - lag + (q + 1) * lag // chunks)
                def _(r):
                    second(2, r)

            @pl.loop(q * tiles // chunks, (q + 1) * tiles // chunks)
            def _(i):
                pl.when(low >= 0)(lambda: hidden_tile(low, i))
                pl.when(jnp.logical_and(d > 0, high < Z))(lambda: hidden_tile(high, i))

    own_scale.wait()

    @pl.loop(1, F)
    def _(s):
        to = lax.rem(f + s, F)
        scale_copy(to, to).wait_recv()

    @pl.loop(0, F)
    def _(src):
        row = lax.broadcasted_iota(jnp.int32, (part, part), 0)
        lane = lax.broadcasted_iota(jnp.int32, (part, part), 1)
        spread = jnp.where(row == lane, scale[src], 0.0)
        weight[pl.ds(pl.multiple_of(src * part, part), part)] = jnp.broadcast_to(
            jnp.sum(spread, axis=1, keepdims=True), (part, weight.shape[1])
        )

    settle(2)

    def strip(q):
        return pl.ds(pl.multiple_of(q * rows, rows), rows)

    def pair_copy(d):
        return remote(comb.at[d, 1 - core], got.at[d], pair_s.at[d], pair_r.at[d], fs=partner)

    def up_copy(d, q):
        return remote(
            comb.at[d, core, strip(q)], above.at[d, strip(q)], up_s.at[d, q], up_r.at[d, q],
            fs=f + 2,
        )

    def dn_copy(d, q):
        return remote(
            comb.at[d, core, strip(q)], above.at[jnp.where(d == z - 1, Z, d), strip(q)], dn_s.at[d, q],
            dn_r.at[d, q],
            fs=f - 2,
        )

    def x_copy(q, tt, src):
        start = pl.multiple_of(src * part + q * rows, rows)
        return remote(
            comb.at[z, core, strip(q), pl.ds(pl.multiple_of(tt * own, own), own)],
            out.at[pl.ds(start, rows)], x_s.at[q, tt], x_r.at[q, src], tp=tt,
        )

    def dest_of(k):
        half = k // 2
        d = jnp.where(lax.rem(k, 2) == 0, Z - 1 - half, half)
        return jnp.where(2 * z < Z, d, Z - 1 - d)

    def add(d, q, extra, e):
        here = comb[d, core, strip(q)].astype(jnp.float32)
        comb[d, core, strip(q)] = (here + extra[e, strip(q)].astype(jnp.float32)).astype(comb.dtype)

    def compute(d):
        tokens = tokens_of(d)
        factor = jnp.concatenate([weight[tokens]] * (tile // weight.shape[1]), axis=1)

        @pl.loop(0, width // tile)
        def _(i):
            tt, col = i // (own // tile), lax.rem(i, own // tile) * tile
            weights = down[
                pl.ds(pl.multiple_of(tt * inner, inner), inner),
                pl.ds(pl.multiple_of(col, tile), tile),
            ]
            value = jnp.dot(hidden[tokens], weights, preferred_element_type=jnp.float32)
            value = (value * factor).astype(comb.dtype)
            comb[d, :, :, pl.ds(pl.multiple_of(i * tile, tile), tile)] = value.reshape(
                2, part, tile
            )

        pair_copy(d).start()

    def paired(d):
        pair_copy(d).wait_recv()

        @pl.loop(0, chunks)
        def _(q):
            add(d, q, got, d)

            @pl.when(jnp.logical_and(z == 0, d > z))
            def _():
                up_copy(d, q).start()

            @pl.when(jnp.logical_and(z == Z - 1, d < z))
            def _():
                dn_copy(d, q).start()

    compute(dest_of(0))

    @pl.loop(1, Z)
    def _(k):
        compute(dest_of(k))
        paired(dest_of(k - 1))

    paired(dest_of(Z - 1))

    ups, downs = 2 * z, 2 * (Z - 1 - z)
    last = jnp.maximum(
        jnp.where(lower, (Z - 1 - z) * chunks + ups, 0), jnp.where(upper, z * chunks + downs, 0)
    )

    @pl.loop(0, Z * chunks + 2 * Z)
    def _(step):
        u, v, w = step - ups, step - downs, step - last
        uq, vq = lax.rem(jnp.maximum(u, 0), chunks), lax.rem(jnp.maximum(v, 0), chunks)
        high, low = Z - 1 - jnp.maximum(u, 0) // chunks, jnp.maximum(v, 0) // chunks

        @pl.when(jnp.logical_and(jnp.logical_and(lower, u >= 0), high >= z))
        def _():
            up_copy(high, uq).wait_recv()
            add(high, uq, above, high)

            @pl.when(high > z)
            def _():
                up_copy(high, uq).start()

        @pl.when(jnp.logical_and(jnp.logical_and(upper, v >= 0), low <= z))
        def _():
            dn_copy(low, vq).wait_recv()
            add(low, vq, above, jnp.where(low == z, Z, low))

            @pl.when(low < z)
            def _():
                dn_copy(low, vq).start()

        @pl.when(jnp.logical_and(w >= 0, w < chunks))
        def _():
            for dt in range(1, T):
                x_copy(w, lax.rem(t + dt, T), t).start()
            start = pl.multiple_of(t * part + w * rows, rows)
            out[pl.ds(start, rows)] = comb[
                z, core, strip(w), pl.ds(pl.multiple_of(t * own, own), own)
            ]

    @pl.loop(0, Z)
    def _(d):
        pair_copy(d).wait_send()

        @pl.loop(0, chunks)
        def _(q):
            @pl.when(jnp.logical_and(upper, d > z))
            def _():
                up_copy(d, q).wait_send()

            @pl.when(jnp.logical_and(lower, d < z))
            def _():
                dn_copy(d, q).wait_send()

    @pl.loop(0, chunks)
    def _(q):
        for dt in range(1, T):
            tt = lax.rem(t + dt, T)
            x_copy(q, tt, t).wait_send()
            x_copy(q, tt, tt).wait_recv()

    for m in range(3):
        sent = mats[m][1].at[pl.ds(0, mats[m][1].shape[0] - mats[m][0].shape[1])]
        remote(sent, sent, send_w.at[m], recv_w.at[m, 0, 0, 0], fs=partner).wait_send()

    @pl.loop(1, F)
    def _(s):
        scale_copy(lax.rem(f + s, F), f).wait_send()

    @pl.loop(0, Z)
    def _(d):
        src = 2 * d + core

        @pl.loop(0, chunks)
        def _(q):
            token_copy(token_rows(src, q), src, q, 2).wait_send()

            @pl.when(jnp.logical_and(d <= z, upper))
            def _():
                token_copy(token_rows(src, q), src, q, 0).wait_send()

            @pl.when(jnp.logical_and(d >= z, lower))
            def _():
                token_copy(token_rows(src, q), src, q, 1).wait_send()


def deliver(T, gate, up, down, mixed, gate_out, up_out, down_out, mixed_out, sems):
    t = lax.axis_index("tp")
    depth, own, width = gate_out.shape[1], down_out.shape[1], down.shape[1]
    deep = pl.ds(pl.multiple_of(t * depth, depth), depth)
    copies = [
        pltpu.make_async_copy(gate.at[deep], gate_out.at[0], sems.at[0]),
        pltpu.make_async_copy(up.at[deep], up_out.at[0], sems.at[1]),
        pltpu.make_async_copy(mixed, mixed_out, sems.at[2]),
    ]
    for tt in range(T):
        source = down.at[pl.ds(pl.multiple_of((tt * T + t) * own, own), own)]
        copies.append(
            pltpu.make_async_copy(
                source, down_out.at[0, :, pl.ds(tt * width, width)], sems.at[3 + tt]
            )
        )
    for copy in copies:
        copy.start()
    for copy in copies:
        copy.wait()


def shards(mesh, prompt, routes, route_weight, norm_gain, gate_train, up_train, down_train):
    G, F, T = (mesh.shape[name] for name in ("grp", "fs", "tp"))
    Z = F // 2
    t = lax.axis_index("tp")
    experts = gate_train.shape[0]
    tok_rows, width = prompt.shape
    part = tok_rows // T
    values = lax.dynamic_slice_in_dim(prompt, t * part, part, 0).astype(jnp.float32)
    normed = (values * lax.rsqrt(jnp.mean(values * values, axis=-1, keepdims=True) + EPS)).astype(
        jnp.bfloat16
    )
    lanes = jnp.arange(experts, dtype=jnp.int32)
    routes = lax.dynamic_slice_in_dim(routes, t * part, part, 0)
    route_weight = lax.dynamic_slice_in_dim(route_weight, t * part, part, 0)
    scale = jnp.sum(
        jnp.where(routes[:, :, None] == lanes[None, None, :], route_weight[:, :, None], 0.0), axis=1
    )

    gain = norm_gain[None, :, None]
    scale = scale.T.reshape(experts, 1, part)
    mats = (
        (gain * gate_train).astype(jnp.bfloat16),
        (gain * up_train).astype(jnp.bfloat16),
        down_train.astype(jnp.bfloat16),
    )
    full = [jax.ShapeDtypeStruct((T * F * w.shape[1], w.shape[2]), w.dtype) for w in mats]
    mixed = jax.ShapeDtypeStruct((tok_rows, width // T), normed.dtype)
    inner = T * mats[0].shape[2]
    chunks = part // chunk_rows(part)
    bf16, f32, dma = jnp.bfloat16, jnp.float32, pltpu.SemaphoreType.DMA
    scratch = 2 * F * part * (4 * width + inner + 256) + part * width * 2
    room = 2 * sum(w.size for w in full + [mixed]) + scratch + 4 * 1024 * 1024
    held = pl.pallas_call(
        functools.partial(layer, (G, F, T)),
        out_shape=full + [mixed],
        in_specs=[pl.BlockSpec(memory_space=pl.ANY)] * 5,
        out_specs=[pl.BlockSpec(memory_space=pltpu.VMEM)] * 4,
        scratch_shapes=[
            pltpu.VMEM((F * part, width), bf16),
            pltpu.VMEM((F * part, inner), bf16),
            pltpu.VMEM((Z, 2, part, width), bf16),
            pltpu.VMEM((Z, part, width), bf16),
            pltpu.VMEM((Z + 1, part, width), bf16),
            pltpu.VMEM((F, 1, part), f32),
            pltpu.VMEM((F * part, 128), f32),
            dma((3, F, G, T)),
            dma((3,)),
            dma((F, chunks)),
            dma((F, chunks)),
            dma((F, chunks)),
            dma((F, chunks)),
            dma((F,)),
            dma((F,)),
            dma((5,)),
            dma((Z,)),
            dma((Z,)),
            dma((Z, chunks)),
            dma((Z, chunks)),
            dma((Z, chunks)),
            dma((Z, chunks)),
            dma((chunks, T)),
            dma((chunks, T)),
        ],
        compiler_params=pltpu.CompilerParams(
            collective_id=0, has_side_effects=True, vmem_limit_bytes=min(room, 63 * 1024 * 1024)
        ),
    )(scale, normed, *mats)
    return pl.pallas_call(
        functools.partial(deliver, T),
        out_shape=[
            jax.ShapeDtypeStruct((1, full[0].shape[0] // T, full[0].shape[1]), bf16),
            jax.ShapeDtypeStruct((1, full[1].shape[0] // T, full[1].shape[1]), bf16),
            jax.ShapeDtypeStruct((1, inner // T, width), bf16),
            mixed,
        ],
        in_specs=[pl.BlockSpec(memory_space=pl.ANY)] * 4,
        out_specs=[pl.BlockSpec(memory_space=pl.ANY)] * 4,
        scratch_shapes=[dma((3 + T,))],
        compiler_params=pltpu.CompilerParams(vmem_limit_bytes=1024 * 1024),
    )(*held)


def solution(mesh):
    return jax.shard_map(
        functools.partial(shards, mesh),
        mesh=mesh,
        in_specs=(
            P(("grp", "fs"), None),
            P(("grp", "fs"), None),
            P(("grp", "fs"), None),
            P("fs"),
            P(None, "fs", "tp"),
            P(None, "fs", "tp"),
            P(None, "fs", "tp"),
        ),
        out_specs=(
            P(("grp", "fs"), None, "tp"),
            P(("grp", "fs"), None, "tp"),
            P(("grp", "fs"), "tp", None),
            P(("grp", "fs"), "tp"),
        ),
        check_vma=False,
    )
```

time: 248 us -> 225 us (0.907)
  matrix products: 19.3 us -> 0 us
  Pallas kernels: 201 us -> 209 us
  local copies, waits for them, and re-layouts: 14.7 us -> 8.18 us
  other arithmetic: 10.1 us -> 6.85 us
    dot_general x4 -> x0, matrix products: 19.3 us -> none  [the longest x2 10.7 us: shards(): gate_pre = jnp.dot(tokens, gate[i], preferred_element_type=jnp.float32)]
    pallas_call x2, Pallas kernels: 201 us -> 209 us  [the longest x1 206 us: shards(): pl.pallas_call(functools.partial(layer, (G, F, T)), out_shape=full + [mix...]
    unnamed x13 -> x14, local copies, waits for them, and re-layouts: 1.07 us -> 7.33 us
    dynamic_slice x1 -> x0, local copies, waits for them, and re-layouts: 4.57 us -> none  [shards(): up_mine = lax.dynamic_slice_in_dim(up, t, 1, 0)]
    reshape x3 -> x1, local copies, waits for them, and re-layouts: 4.28 us -> 0.01 us  [shards(): scale = scale.T.reshape(experts, 1, part)]
    transpose x2 -> x0, local copies, waits for them, and re-layouts: 3.93 us -> none  [shards(): down_mine = down_mine.transpose(1, 0, 2).reshape(1, own, -1)]
    convert_element_type x1, other arithmetic: 4.96 us -> 1.3 us  [shards(): (gain * up_train).astype(jnp.bfloat16)]
where the time goes in v2:
time: 225 us
  Pallas kernels  209 us (93%)
  local copies, waits for them, and re-layouts  8.18 us (4%)
  other arithmetic  6.85 us (3%)
    pallas_call x1, Pallas kernels, shards(): pl.pallas_call(functools.partial(layer, (G, F, T)), out_shape=full + [mix...  206 us
    unnamed x14, local copies, waits for them, and re-layouts  7.33 us

profile of v2, /device:TPU:8, one launch (start us, length us, event | category | flops | bytes accessed | tf_op | source)
XLA Modules:
  0.0 224.7 jit_solution(2750070807936149624)
XLA Ops:
  0.6 0.0 copy-start
  0.7 0.0 copy-start.5
  0.7 1.5 fusion
  2.2 0.0 copy-done
  2.2 0.1 constant_dynamic-slice_fusion.1
  2.3 0.8 constant_dynamic-slice_fusion
  3.1 1.3 fusion.1.tok_in
  4.4 0.0 copy-start.4
  4.4 0.0 copy-start.6
  4.4 2.7 %convert_element_type.19.down_in = bf16[8,128,1024]{2,1,0:T(8,128)(2,1)S(1)} convert(f32[8,128,1024]{2,1,0:T(8,128)} %param.13) | non-fusion elementwise | flops 1048576 | bytes 6291456 | tf_op jit(solution)/shard_map/convert_element_type | solution.py:545
  7.1 0.0 copy-done.5
  7.1 0.7 copy-done.4
  7.9 0.0 copy-done.6
  7.9 1.3 multiply_convert_fusion
  9.2 206.1 %shard_map.102 = (bf16[4096,512]{1,0:T(8,128)(2,1)}, bf16[4096,512]{1,0:T(8,128)(2,1)}, bf16[2048,1024]{1,0:T(8,128)(2,1)}, bf16[384,1024]{1,0:T(8,128)(2,1)S(1)}) custom-call(f32[8,1,192]{2,1,0:T(1,128)S(1)} %reshape.22.scale_in, bf16[192,2048]{1,0:T(8,128)(2,1)S(1)} %fusion.1.tok_in, bf16[8,256,512]{2,1,0:T(8,128)(2,1)S(1)} %get-tuple-element.13.gate_in, ...), custom_call_target="tpu_custom_call" | custom-call | tf_op jit(solution)/shard_map/pallas_call | solution.py:554
  215.2 0.0 copy-start.1
  215.2 2.2 copy-done.1
  217.4 0.0 copy-start.2
  217.4 2.2 copy-done.2
  219.6 0.0 copy-start.3
  219.6 2.2 copy-done.3
  221.8 2.9 %shard_map.103 = (bf16[1,2048,512]{2,1,0:T(8,128)(2,1)}, bf16[1,2048,512]{2,1,0:T(8,128)(2,1)}, bf16[1,512,2048]{2,1,0:T(8,128)(2,1)}, bf16[384,1024]{1,0:T(8,128)(2,1)}) custom-call(bf16[4096,512]{1,0:T(8,128)(2,1)S(1)} %copy-done.1, bf16[4096,512]{1,0:T(8,128)(2,1)S(1)} %copy-done.2, bf16[2048,1024]{1,0:T(8,128)(2,1)S(1)} %copy-done.3, ...), custom_call_target="tpu_custom_call" | custom-call | tf_op jit(solution)/shard_map/pallas_call | solution.py:589
  (3 shorter events, 0.0 us)
Async XLA Ops:
  0.6 1.6 copy-start
  0.7 6.5 %copy-start.5 = (f32[8,256,512]{2,1,0:T(8,128)S(1)}, f32[8,256,512]{2,1,0:T(8,128)}, u32[]{:S(2)}) copy-start(f32[8,256,512]{2,1,0:T(8,128)} %param.11) | copy-start | bytes 12582916
  4.4 3.5 %copy-start.4 = (f32[8,256,512]{2,1,0:T(8,128)S(1)}, f32[8,256,512]{2,1,0:T(8,128)}, u32[]{:S(2)}) copy-start(f32[8,256,512]{2,1,0:T(8,128)} %param.12) | copy-start | bytes 12582916
  4.4 3.4 %copy-start.6 = (f32[256]{0:T(256)S(1)}, f32[256]{0:T(256)}, u32[]{:S(2)}) copy-start(f32[256]{0:T(256)} %param.10) | copy-start | bytes 3076
  215.2 2.2 copy-start.1
  217.4 2.2 copy-start.2
  219.6 2.2 copy-start.3

commit v3 on v2

v3 whole, which is shorter than its diff:
```python
import functools

import jax
import jax.numpy as jnp
from jax import lax
from jax.experimental import pallas as pl
from jax.experimental.pallas import tpu as pltpu
from jax.sharding import PartitionSpec as P

LIMIT = 7.0
ALPHA = 1.702
EPS = 1e-06
MESH = pl.DeviceIdType.MESH


def chunk_rows(rows):
    return 48 if rows % 48 == 0 else rows


def layer(
    sizes,
    scale_in,
    prompt,
    gain_in,
    gate_in,
    up_in,
    down_in,
    gate,
    up,
    down,
    out,
    tok,
    hidden,
    comb,
    pair,
    got,
    above,
    scale,
    weight,
    gain,
    ready_g,
    ready_u,
    ready_d,
    raw_g,
    raw_u,
    raw_d,
    raw_s,
    recv_w,
    send_w,
    recv_t,
    send_up,
    send_dn,
    send_pt,
    recv_s,
    send_s,
    local,
    pair_s,
    pair_r,
    up_s,
    up_r,
    dn_s,
    dn_r,
    x_s,
    x_r,
):
    G, F, T = sizes
    g, f, t = lax.axis_index("grp"), lax.axis_index("fs"), lax.axis_index("tp")
    Z = F // 2
    z, core = f // 2, lax.rem(f, 2)
    partner = f + 1 - 2 * core
    lower, upper = z > 0, z < Z - 1
    part, width = tok.shape[0] // F, tok.shape[1]
    own = width // T
    rows = chunk_rows(part)
    chunks = part // rows
    inner = hidden.shape[1]
    tile = got.shape[3]
    parts = width // tile
    per_own = own // tile
    cols = gate.shape[1]
    strips = min(256, cols)
    tiles = inner // strips
    far = F - 2
    lag = far // 2

    barrier = pltpu.get_barrier_semaphore()
    for axis, here, count in (("fs", f, F), ("grp", g, G), ("tp", t, T)):
        for s in range(1, count):
            pl.semaphore_signal(
                barrier, inc=1, device_id={axis: lax.rem(here + s, count)}, device_id_type=MESH
            )
    pl.semaphore_wait(barrier, F + G + T - 3)

    def remote(src, dst, send, recv, **where):
        return pltpu.make_async_remote_copy(
            src_ref=src, dst_ref=dst, send_sem=send, recv_sem=recv, device_id=where,
            device_id_type=MESH,
        )

    mats = ((ready_g, gate), (ready_u, up), (ready_d, down))
    trained = ((gate_in, raw_g), (up_in, raw_u), (down_in, raw_d))
    slots = raw_g.shape[0]

    def block_rows(m, src, tt):
        block = mats[m][0].shape[1]
        return mats[m][1].at[pl.ds(pl.multiple_of((tt * F + src) * block, block), block)]

    def piece_rows(m, src, gg, tt):
        block = mats[m][0].shape[1]
        piece = block // G
        start = (tt * F + src) * block + gg * piece
        return mats[m][1].at[pl.ds(pl.multiple_of(start, piece), piece)]

    def sent_piece(m, expert):
        piece = mats[m][0].shape[1] // G
        return mats[m][0].at[expert, pl.ds(pl.multiple_of(g * piece, piece), piece)]

    def wait_piece(m, src, gg, tt):
        ref = piece_rows(m, src, gg, tt)
        remote(ref, ref, send_w.at[m], recv_w.at[m, src, gg, tt], fs=partner).wait_recv()

    def pass_piece(m, src, gg, tt, **where):
        ref = piece_rows(m, src, gg, tt)
        remote(ref, ref, send_w.at[m], recv_w.at[m, src, gg, tt], **where).start()

    def wait_block(m, src, tt):
        ref = block_rows(m, src, tt)
        remote(ref, ref, send_w.at[m], recv_w.at[m, src, 0, tt], fs=partner).wait_recv()

    def near_blocks(m, src_ref, src):
        for dt in range(1, T):
            remote(
                src_ref, block_rows(m, src, t), send_w.at[m], recv_w.at[m, src, 0, t],
                tp=lax.rem(t + dt, T),
            ).start()

    both = jnp.minimum(z, Z - 1 - z)
    rising = jnp.where(2 * z < Z, 1, -1)

    def far_peer(r):
        k, side = r // 2, lax.rem(r, 2)
        near = (k // 2 + 1) * (2 * lax.rem(k, 2) - 1)
        chip = z + rising * jnp.where(k < 2 * both, near, k - both + 1)
        return 2 * chip + jnp.where(side == 0, core, 1 - core)

    def token_block(src):
        return tok.at[pl.ds(pl.multiple_of(src * part, part), part)]

    def token_rows(src, q):
        return tok.at[pl.ds(pl.multiple_of(src * part + q * rows, rows), rows)]

    own_tokens = pltpu.make_async_copy(
        prompt.at[pl.ds(pl.multiple_of(t * part, part), part)], token_block(f), local.at[0]
    )
    own_scale = pltpu.make_async_copy(scale_in.at[f], scale.at[f], local.at[1])

    def scale_copy(to, src):
        return remote(scale_in.at[to], scale.at[src], send_s.at[to], recv_s.at[src], fs=to)

    def token_copy(src_ref, src, q, kind):
        sems, to = ((send_up, f + 2), (send_dn, f - 2), (send_pt, partner))[kind]
        return remote(src_ref, token_rows(src, q), sems.at[src, q], recv_t.at[src, q], fs=to)

    def column(values):
        size = values.shape[1]
        row = lax.broadcasted_iota(jnp.int32, (size, size), 0)
        lane = lax.broadcasted_iota(jnp.int32, (size, size), 1)
        spread = jnp.where(row == lane, values, 0.0)
        return jnp.broadcast_to(jnp.sum(spread, axis=1, keepdims=True), (size, 128))

    def expert_of(i):
        return jnp.where(i == 0, partner, jnp.where(i == 1, f, far_peer(jnp.maximum(i - 2, 0))))

    def load(m, i):
        slot = lax.rem(i, slots)
        return pltpu.make_async_copy(
            trained[m][0].at[expert_of(i)], trained[m][1].at[slot], raw_s.at[m, slot]
        )

    for m in range(3):
        pl.loop(0, min(slots, F))(lambda i, m=m: load(m, i).start())

    def convert(m, i):
        load(m, i).wait()
        value = trained[m][1][lax.rem(i, slots)]
        if m < 2:
            value = value * jnp.concatenate([gain[...]] * (value.shape[1] // 128), axis=1)
        value = value.astype(mats[m][0].dtype)
        mats[m][0][expert_of(i)] = value
        block = value.shape[0]

        @pl.when(i == 1)
        def _():
            start = pl.multiple_of((t * F + f) * block, block)
            mats[m][1][pl.ds(start, block)] = value

        pl.when(i + slots < F)(lambda: load(m, i + slots).start())

    def send_piece(m, r):
        to = far_peer(r)
        remote(
            sent_piece(m, to), piece_rows(m, f, g, t), send_w.at[m], recv_w.at[m, f, g, t], fs=to
        ).start()

    def emit(m, i):
        @pl.when(i == 0)
        def _():
            remote(
                mats[m][0].at[partner], block_rows(m, f, t), send_w.at[m], recv_w.at[m, f, 0, t],
                fs=partner,
            ).start()

        if m == 0:
            pl.when(i == 1)(lambda: near_blocks(0, mats[0][0].at[f], f))
            pl.when(i > 1)(lambda: send_piece(m, i - 2))

    def send_tokens(q):
        source = token_rows(f, q)
        pl.when(upper)(lambda: token_copy(source, f, q, 0).start())
        pl.when(lower)(lambda: token_copy(source, f, q, 1).start())
        token_copy(source, f, q, 2).start()

    own_scale.start()
    own_tokens.start()

    @pl.loop(1, F)
    def _(s):
        scale_copy(lax.rem(f + s, F), f).start()

    gain[...] = column(gain_in[...])
    for m in range(3):

        @pl.loop(0, F + 1)
        def _(i, m=m):
            pl.when(i < F)(lambda: convert(m, i))
            pl.when(i > 0)(lambda: emit(m, i - 1))

    own_tokens.wait()

    @pl.loop(0, chunks)
    def _(q):
        where = pl.ds(pl.multiple_of(f * part + q * rows, rows), rows)
        values = tok[where].astype(jnp.float32)
        mean = jnp.mean(values * values, axis=-1, keepdims=True)
        tok[where] = (values * lax.rsqrt(mean + EPS)).astype(tok.dtype)

    def first(m, r):
        src = far_peer(r)
        wait_piece(m, src, g, t)
        for dg in range(1, G):
            pass_piece(m, src, g, t, grp=lax.rem(g + dg, G))
        for dt in range(1, T):
            pass_piece(m, src, g, t, tp=lax.rem(t + dt, T))

    def second(m, r):
        src = far_peer(r)
        across = lax.rem(r, 6) == 0
        for dg in range(1, G):
            gg = lax.rem(g + dg, G)
            wait_piece(m, src, gg, t)

            @pl.when(across)
            def _():
                for dt in range(1, T):
                    pass_piece(m, src, gg, t, tp=lax.rem(t + dt, T))

        for dt in range(1, T):
            tt = lax.rem(t + dt, T)
            wait_piece(m, src, g, tt)

            @pl.when(jnp.logical_not(across))
            def _():
                for dg in range(1, G):
                    pass_piece(m, src, g, tt, grp=lax.rem(g + dg, G))

    def settle(m):
        @pl.loop(0, far)
        def _(r):
            for dg in range(1, G):
                for dt in range(1, T):
                    wait_piece(m, far_peer(r), lax.rem(g + dg, G), lax.rem(t + dt, T))

        for src in (f, partner):
            for dt in range(1, T):
                wait_block(m, src, lax.rem(t + dt, T))

    def chain(d, q):
        @pl.when(z >= d)
        def _():
            src = f - 2 * d
            token_copy(token_rows(src, q), src, q, 2).wait_recv()

            @pl.when(upper)
            def _():
                token_copy(token_rows(src, q), src, q, 0).start()

            token_copy(token_rows(src, q), src, q, 2).start()

        @pl.when(z + d < Z)
        def _():
            src = f + 2 * d
            token_copy(token_rows(src, q), src, q, 2).wait_recv()

            @pl.when(lower)
            def _():
                token_copy(token_rows(src, q), src, q, 1).start()

            token_copy(token_rows(src, q), src, q, 2).start()

    def tokens_of(d):
        return pl.ds(pl.multiple_of(d * 2 * part, 2 * part), 2 * part)

    def partner_tokens(d):
        src = 2 * d + 1 - core

        @pl.loop(0, chunks)
        def _(q):
            token_copy(token_rows(src, q), src, q, 2).wait_recv()

    def hidden_tile(d, i):
        per = cols // strips
        tt, col = i // per, lax.rem(i, per) * strips
        where = (
            pl.ds(pl.multiple_of(tt * width, width), width),
            pl.ds(pl.multiple_of(col, strips), strips),
        )
        held = tok[tokens_of(d)]
        gate_pre = jnp.dot(held, gate[where], preferred_element_type=jnp.float32)
        up_pre = jnp.dot(held, up[where], preferred_element_type=jnp.float32)
        gate_pre = jnp.minimum(gate_pre, LIMIT)
        up_pre = jnp.clip(up_pre, -LIMIT, LIMIT)
        value = (up_pre + 1.0) * gate_pre * jax.nn.sigmoid(ALPHA * gate_pre)
        hidden[tokens_of(d), pl.ds(pl.multiple_of(i * strips, strips), strips)] = value.astype(
            hidden.dtype
        )

    def span(i, count, total):
        return pl.loop(i * total // count, (i + 1) * total // count)

    for m in range(3):
        if m > 0:
            near_blocks(m, mats[m][0].at[f], f)
        if m == 2:
            pl.loop(far - lag, far)(lambda r: second(1, r))
            pl.loop(0, chunks)(lambda q: chain(1, q))

        @pl.loop(0, far)
        def _(r, m=m):
            first(m, r)
            if m == 0:
                send_piece(1, r)

            @pl.when(r >= lag)
            def _():
                second(m, r - lag)

            if m == 1:

                @pl.when(r < lag)
                def _():
                    second(m - 1, far - lag + r)

            if m == 1:

                @pl.when(r < lag)
                def _():
                    span(r, lag, chunks)(send_tokens)

                @pl.when(r >= lag)
                def _():
                    span(r - lag, far - lag, far)(lambda k: send_piece(2, k))

            if m == 2:

                @pl.when(r == lag)
                def _():
                    partner_tokens(z)
                    settle(0)
                    settle(1)

                @pl.when(r >= lag)
                def _():
                    span(r - lag, far - lag, tiles)(lambda i: hidden_tile(z, i))

        wait_block(m, partner, t)
        near_blocks(m, block_rows(m, partner, t), partner)

    def pair_copy(d, q, slot):
        return remote(
            pair.at[slot, 1 - core], got.at[d, q], pair_s.at[slot], pair_r.at[d, q], fs=partner
        )

    def up_copy(d, q):
        return remote(
            comb.at[d, q], above.at[d, q], up_s.at[d, q], up_r.at[d, q], fs=f + 2
        )

    def dn_copy(d, q):
        return remote(
            comb.at[d, q], above.at[jnp.where(d == z - 1, Z, d), q], dn_s.at[d, q],
            dn_r.at[d, q], fs=f - 2,
        )

    def home(src, q):
        return (
            pl.ds(pl.multiple_of(src * part, part), part),
            pl.ds(pl.multiple_of(lax.rem(q, per_own) * tile, tile), tile),
        )

    def owner(q):
        return lax.rem(t + 1 + q // per_own, T)

    def x_copy(q, to, src):
        return remote(
            comb.at[z, q], out.at[home(src, q)], x_s.at[q],
            x_r.at[lax.rem(q, per_own), src], tp=to,
        )

    def up_dest(k):
        return jnp.where(k < 2, Z - 2 + k, Z - 1 - k)

    def dest_of(k):
        d = jnp.where(k == Z - 1, 0, up_dest(k))
        return jnp.where(2 * z < Z, d, Z - 1 - d)

    def add(d, q, extra, e):
        here = comb[d, q].astype(jnp.float32)
        comb[d, q] = (here + extra[e, q].astype(jnp.float32)).astype(comb.dtype)

    def compute(d, q, slot):
        tokens = tokens_of(d)
        factor = jnp.concatenate([weight[tokens]] * (tile // weight.shape[1]), axis=1)
        weights = down[
            pl.ds(pl.multiple_of(owner(q) * inner, inner), inner),
            pl.ds(pl.multiple_of(lax.rem(q, per_own) * tile, tile), tile),
        ]
        value = jnp.dot(hidden[tokens], weights, preferred_element_type=jnp.float32)
        pair[slot] = (value * factor).astype(comb.dtype).reshape(2, part, tile)
        pair_copy(d, q, slot).start()

    def paired(d, q, slot):
        pair_copy(d, q, slot).wait()
        here = pair[slot, core].astype(jnp.float32)
        comb[d, q] = (here + got[d, q].astype(jnp.float32)).astype(comb.dtype)

        @pl.when(jnp.logical_and(z == 0, d > z))
        def _():
            up_copy(d, q).start()

        @pl.when(jnp.logical_and(z == Z - 1, d < z))
        def _():
            dn_copy(d, q).start()

    late = 2
    edge = jnp.logical_or(z == 0, z == Z - 1)

    def partials(low, high):
        @pl.loop(low, high + late)
        def _(n):
            @pl.when(n < high)
            def _():
                compute(dest_of(n // parts), lax.rem(n, parts), lax.rem(n, 4))

            @pl.when(n >= low + late)
            def _():
                k = n - late
                paired(dest_of(k // parts), lax.rem(k, parts), lax.rem(k, 4))

    def settle_down():
        own_scale.wait()

        @pl.loop(1, F)
        def _(s):
            to = lax.rem(f + s, F)
            scale_copy(to, to).wait_recv()

        @pl.loop(0, F)
        def _(src):
            weight[pl.ds(pl.multiple_of(src * part, part), part)] = column(scale[src])

        settle(2)

    @pl.loop(1, Z)
    def _(d):
        low, high = z - d, z + d

        @pl.when(d == Z - 1)
        def _():
            settle_down()
            pl.when(edge)(lambda: partials(0, parts))

        pl.when(low >= 0)(lambda: partner_tokens(low))
        pl.when(high < Z)(lambda: partner_tokens(high))

        @pl.loop(0, chunks)
        def _(q):
            pl.when(d + 1 < Z)(lambda: chain(d + 1, q))

            @pl.when(d == 1)
            def _():
                span(q, chunks, lag)(lambda r: second(2, far - lag + r))

            @span(q, chunks, tiles)
            def _(i):
                pl.when(low >= 0)(lambda: hidden_tile(low, i))
                pl.when(high < Z)(lambda: hidden_tile(high, i))

    partials(jnp.where(edge, parts, 0), Z * parts)

    ups, downs = 2 * z, 2 * (Z - 1 - z)
    def turn(rank):
        first_two = rank - (Z - 2)
        return jnp.where(first_two >= 0, first_two, Z - 1 - rank) * parts + 2 * rank

    last = jnp.maximum(jnp.where(lower, turn(z), 0), jnp.where(upper, turn(Z - 1 - z), 0))

    @pl.loop(0, Z * parts + 2 * Z)
    def _(step):
        u, v, w = step - ups, step - downs, step - last
        uq, vq = lax.rem(jnp.maximum(u, 0), parts), lax.rem(jnp.maximum(v, 0), parts)
        high = up_dest(jnp.maximum(u, 0) // parts)
        low = Z - 1 - up_dest(jnp.maximum(v, 0) // parts)
        going = (Z - 1) * parts

        @pl.when(lower & (u >= 0) & (u < going) & (high >= z))
        def _():
            up_copy(high, uq).wait_recv()
            add(high, uq, above, high)

            @pl.when(high > z)
            def _():
                up_copy(high, uq).start()

        @pl.when(upper & (v >= 0) & (v < going) & (low <= z))
        def _():
            dn_copy(low, vq).wait_recv()
            add(low, vq, above, jnp.where(low == z, Z, low))

            @pl.when(low < z)
            def _():
                dn_copy(low, vq).start()

        @pl.when(jnp.logical_and(w >= 0, w < parts))
        def _():
            @pl.when(w < parts - per_own)
            def _():
                x_copy(w, owner(w), t).start()

            @pl.when(w >= parts - per_own)
            def _():
                out[home(t, w)] = comb[z, w]

    @pl.loop(0, Z)
    def _(d):
        @pl.loop(0, parts)
        def _(q):
            @pl.when(jnp.logical_and(upper, d > z))
            def _():
                up_copy(d, q).wait_send()

            @pl.when(jnp.logical_and(lower, d < z))
            def _():
                dn_copy(d, q).wait_send()

    @pl.loop(0, parts - per_own)
    def _(q):
        x_copy(q, owner(q), t).wait_send()
        x_copy(q, owner(q), owner(q)).wait_recv()

    for m in range(3):
        sent = mats[m][1].at[pl.ds(0, mats[m][1].shape[0] - mats[m][0].shape[1])]
        remote(sent, sent, send_w.at[m], recv_w.at[m, 0, 0, 0], fs=partner).wait_send()

    @pl.loop(1, F)
    def _(s):
        scale_copy(lax.rem(f + s, F), f).wait_send()

    @pl.loop(0, Z)
    def _(d):
        src = 2 * d + core

        @pl.loop(0, chunks)
        def _(q):
            token_copy(token_rows(src, q), src, q, 2).wait_send()

            @pl.when(jnp.logical_and(d <= z, upper))
            def _():
                token_copy(token_rows(src, q), src, q, 0).wait_send()

            @pl.when(jnp.logical_and(d >= z, lower))
            def _():
                token_copy(token_rows(src, q), src, q, 1).wait_send()


def deliver(T, gate, up, down, mixed, gate_out, up_out, down_out, mixed_out, sems):
    t = lax.axis_index("tp")
    depth, own, width = gate_out.shape[1], down_out.shape[1], down.shape[1]
    deep = pl.ds(pl.multiple_of(t * depth, depth), depth)
    copies = [
        pltpu.make_async_copy(gate.at[deep], gate_out.at[0], sems.at[0]),
        pltpu.make_async_copy(up.at[deep], up_out.at[0], sems.at[1]),
        pltpu.make_async_copy(mixed, mixed_out, sems.at[2]),
    ]
    for tt in range(T):
        source = down.at[pl.ds(pl.multiple_of((tt * T + t) * own, own), own)]
        copies.append(
            pltpu.make_async_copy(
                source, down_out.at[0, :, pl.ds(tt * width, width)], sems.at[3 + tt]
            )
        )
    for copy in copies:
        copy.start()
    for copy in copies:
        copy.wait()


def shards(mesh, prompt, routes, route_weight, norm_gain, gate_train, up_train, down_train):
    G, F, T = (mesh.shape[name] for name in ("grp", "fs", "tp"))
    Z = F // 2
    t = lax.axis_index("tp")
    experts = gate_train.shape[0]
    tok_rows, width = prompt.shape
    part = tok_rows // T
    lanes = jnp.arange(experts, dtype=jnp.int32)
    routes = lax.dynamic_slice_in_dim(routes, t * part, part, 0)
    route_weight = lax.dynamic_slice_in_dim(route_weight, t * part, part, 0)
    scale = jnp.sum(
        jnp.where(routes[:, :, None] == lanes[None, None, :], route_weight[:, :, None], 0.0), axis=1
    )

    scale = scale.T.reshape(experts, 1, part)
    mats = (gate_train, up_train, down_train)
    full = [jax.ShapeDtypeStruct((T * F * w.shape[1], w.shape[2]), jnp.bfloat16) for w in mats]
    mixed = jax.ShapeDtypeStruct((tok_rows, width // T), jnp.bfloat16)
    inner = T * mats[0].shape[2]
    tile = min(512, width // T)
    parts = width // tile
    chunks = part // chunk_rows(part)
    bf16, f32, dma = jnp.bfloat16, jnp.float32, pltpu.SemaphoreType.DMA
    slots = min(4, F)
    scratch = F * part * (5 * width + 2 * inner + 512) + part * width * 6
    scratch += sum(2 * w.size + 4 * slots * w[0].size for w in mats)
    results = 2 * sum(w.size for w in full + [mixed])
    room = scratch + 6 * 1024 * 1024
    if room + results > 56 * 1024 * 1024:
        room += results
    held = pl.pallas_call(
        functools.partial(layer, (G, F, T)),
        out_shape=full + [mixed],
        in_specs=[pl.BlockSpec(memory_space=pl.ANY)] * 2
        + [pl.BlockSpec(memory_space=pltpu.VMEM)]
        + [pl.BlockSpec(memory_space=pl.ANY)] * 3,
        out_specs=[pl.BlockSpec(memory_space=pltpu.VMEM)] * 4,
        scratch_shapes=[
            pltpu.VMEM((F * part, width), bf16),
            pltpu.VMEM((F * part, inner), bf16),
            pltpu.VMEM((Z, parts, part, tile), bf16),
            pltpu.VMEM((4, 2, part, tile), bf16),
            pltpu.VMEM((Z, parts, part, tile), bf16),
            pltpu.VMEM((Z + 1, parts, part, tile), bf16),
            pltpu.VMEM((F, 1, part), f32),
            pltpu.VMEM((F * part, 128), f32),
            pltpu.VMEM((mats[0].shape[1], 128), f32),
            *[pltpu.VMEM(w.shape, bf16) for w in mats],
            *[pltpu.VMEM((slots,) + w.shape[1:], f32) for w in mats],
            dma((3, slots)),
            dma((3, F, G, T)),
            dma((3,)),
            dma((F, chunks)),
            dma((F, chunks)),
            dma((F, chunks)),
            dma((F, chunks)),
            dma((F,)),
            dma((F,)),
            dma((2,)),
            dma((4,)),
            dma((Z, parts)),
            dma((Z, parts)),
            dma((Z, parts)),
            dma((Z, parts)),
            dma((Z, parts)),
            dma((parts,)),
            dma((parts // T, T)),
        ],
        compiler_params=pltpu.CompilerParams(
            collective_id=0, has_side_effects=True, vmem_limit_bytes=min(room, 63 * 1024 * 1024)
        ),
    )(scale, prompt, norm_gain.reshape(1, -1), *mats)
    return pl.pallas_call(
        functools.partial(deliver, T),
        out_shape=[
            jax.ShapeDtypeStruct((1, full[0].shape[0] // T, full[0].shape[1]), bf16),
            jax.ShapeDtypeStruct((1, full[1].shape[0] // T, full[1].shape[1]), bf16),
            jax.ShapeDtypeStruct((1, inner // T, width), bf16),
            mixed,
        ],
        in_specs=[pl.BlockSpec(memory_space=pl.ANY)] * 4,
        out_specs=[pl.BlockSpec(memory_space=pl.ANY)] * 4,
        scratch_shapes=[dma((3 + T,))],
        compiler_params=pltpu.CompilerParams(vmem_limit_bytes=1024 * 1024),
    )(*held)


def solution(mesh):
    return jax.shard_map(
        functools.partial(shards, mesh),
        mesh=mesh,
        in_specs=(
            P(("grp", "fs"), None),
            P(("grp", "fs"), None),
            P(("grp", "fs"), None),
            P("fs"),
            P(None, "fs", "tp"),
            P(None, "fs", "tp"),
            P(None, "fs", "tp"),
        ),
        out_specs=(
            P(("grp", "fs"), None, "tp"),
            P(("grp", "fs"), None, "tp"),
            P(("grp", "fs"), "tp", None),
            P(("grp", "fs"), "tp"),
        ),
        check_vma=False,
    )
```

time: 225 us -> 186 us (0.83); the launches traced: 225 us -> 183 us
  Pallas kernels: 209 us -> 179 us
  other arithmetic: 6.85 us -> 0.01 us
  local copies, waits for them, and re-layouts: 8.18 us -> 3.61 us
    pallas_call x1, Pallas kernels: 206 us -> 176 us  [shards(): pl.pallas_call(functools.partial(layer, (G, F, T)), out_shape=full + [mix...]
    convert_element_type x3 -> x0, other arithmetic: 5.3 us -> none  [the longest x1 2.66 us: shards(): down_train.astype(jnp.bfloat16)]
    unnamed x14 -> x6, local copies, waits for them, and re-layouts: 7.33 us -> 2.77 us
where the time goes in v3:
time: 186 us; the launch traced here: 183 us
  Pallas kernels  179 us (96%)
  local copies, waits for them, and re-layouts  3.61 us (2%)
    pallas_call x1, Pallas kernels, shards(): pl.pallas_call(functools.partial(layer, (G, F, T)), out_shape=full + [mix...  176 us

profile of v3, /device:TPU:8, one launch (start us, length us, event | category | flops | bytes accessed | tf_op | source)
XLA Modules:
  0.0 183.1 jit_solution(8091177751250179745)
XLA Ops:
  0.6 0.0 copy-start
  0.6 0.7 copy-done
  1.3 0.1 constant_dynamic-slice_fusion.1
  1.4 0.8 constant_dynamic-slice_fusion
  2.2 0.0 copy-start.1
  2.2 1.4 copy-done.1
  3.6 0.0 copy-start.2
  3.6 0.7 copy-done.2
  4.3 175.8 %shard_map.102 = (bf16[4096,512]{1,0:T(8,128)(2,1)S(1)}, bf16[4096,512]{1,0:T(8,128)(2,1)S(1)}, bf16[2048,1024]{1,0:T(8,128)(2,1)S(1)}, bf16[384,1024]{1,0:T(8,128)(2,1)S(1)}) custom-call(f32[8,1,192]{2,1,0:T(1,128)S(1)} %reshape.16.scale_in, bf16[384,2048]{1,0:T(8,128)(2,1)S(1)} %copy-done.1, f32[1,256]{1,0:T(1,128)S(1)} %bitcast.2, ...), custom_call_target="tpu_custom_call" | custom-call | tf_op jit(solution)/shard_map/pallas_call | solution.py:647
  180.1 3.0 %shard_map.103 = (bf16[1,2048,512]{2,1,0:T(8,128)(2,1)}, bf16[1,2048,512]{2,1,0:T(8,128)(2,1)}, bf16[1,512,2048]{2,1,0:T(8,128)(2,1)}, bf16[384,1024]{1,0:T(8,128)(2,1)}) custom-call(bf16[4096,512]{1,0:T(8,128)(2,1)S(1)} %get-tuple-element.8.gate, bf16[4096,512]{1,0:T(8,128)(2,1)S(1)} %get-tuple-element.9.up, bf16[2048,1024]{1,0:T(8,128)(2,1)S(1)} %get-tuple-element.10.down, ...), custom_call_target="tpu_custom_call" | custom-call | tf_op jit(solution)/shard_map/pallas_call | solution.py:689
  (2 shorter events, 0.0 us)
Async XLA Ops:
  0.6 0.7 copy-start
  2.2 1.4 copy-start.1
  3.6 0.7 copy-start.2

commit v4 on v3

--- a/solution.py
+++ b/solution.py
@@ -340,6 +340,18 @@
     for m in range(3):
         if m > 0:
             near_blocks(m, mats[m][0].at[f], f)
+        if m == 1:
+            own_scale.wait()
+
+            @pl.loop(1, F)
+            def _(s):
+                to = lax.rem(f + s, F)
+                scale_copy(to, to).wait_recv()
+
+            @pl.loop(0, F)
+            def _(src):
+                weight[pl.ds(pl.multiple_of(src * part, part), part)] = column(scale[src])
+
         if m == 2:
             pl.loop(far - lag, far)(lambda r: second(1, r))
             pl.loop(0, chunks)(lambda q: chain(1, q))
@@ -466,27 +478,13 @@
                 k = n - late
                 paired(dest_of(k // parts), lax.rem(k, parts), lax.rem(k, 4))
 
-    def settle_down():
-        own_scale.wait()
-
-        @pl.loop(1, F)
-        def _(s):
-            to = lax.rem(f + s, F)
-            scale_copy(to, to).wait_recv()
-
-        @pl.loop(0, F)
-        def _(src):
-            weight[pl.ds(pl.multiple_of(src * part, part), part)] = column(scale[src])
-
-        settle(2)
-
     @pl.loop(1, Z)
     def _(d):
         low, high = z - d, z + d
 
         @pl.when(d == Z - 1)
         def _():
-            settle_down()
+            settle(2)
             pl.when(edge)(lambda: partials(0, parts))
 
         pl.when(low >= 0)(lambda: partner_tokens(low))

time: 186 us -> 186 us (level)
  no operation moved by 1% of the time
where the time goes in v4:
time: 186 us; the launch traced here: 183 us
  Pallas kernels  179 us (96%)
  local copies, waits for them, and re-layouts  3.61 us (2%)
    pallas_call x1, Pallas kernels, shards(): pl.pallas_call(functools.partial(layer, (G, F, T)), out_shape=full + [mix...  176 us

profile of v4, /device:TPU:8, one launch (start us, length us, event | category | flops | bytes accessed | tf_op | source)
XLA Modules:
  0.0 183.0 jit_solution(15538484544863405782)
XLA Ops:
  0.6 0.0 copy-start
  0.6 0.7 copy-done
  1.3 0.1 constant_dynamic-slice_fusion.1
  1.4 0.8 constant_dynamic-slice_fusion
  2.2 0.0 copy-start.1
  2.2 1.4 copy-done.1
  3.6 0.0 copy-start.2
  3.6 0.7 copy-done.2
  4.3 175.8 %shard_map.102 = (bf16[4096,512]{1,0:T(8,128)(2,1)S(1)}, bf16[4096,512]{1,0:T(8,128)(2,1)S(1)}, bf16[2048,1024]{1,0:T(8,128)(2,1)S(1)}, bf16[384,1024]{1,0:T(8,128)(2,1)S(1)}) custom-call(f32[8,1,192]{2,1,0:T(1,128)S(1)} %reshape.16.scale_in, bf16[384,2048]{1,0:T(8,128)(2,1)S(1)} %copy-done.1, f32[1,256]{1,0:T(1,128)S(1)} %bitcast.2, ...), custom_call_target="tpu_custom_call" | custom-call | tf_op jit(solution)/shard_map/pallas_call | solution.py:645
  180.1 3.0 %shard_map.103 = (bf16[1,2048,512]{2,1,0:T(8,128)(2,1)}, bf16[1,2048,512]{2,1,0:T(8,128)(2,1)}, bf16[1,512,2048]{2,1,0:T(8,128)(2,1)}, bf16[384,1024]{1,0:T(8,128)(2,1)}) custom-call(bf16[4096,512]{1,0:T(8,128)(2,1)S(1)} %get-tuple-element.8.gate, bf16[4096,512]{1,0:T(8,128)(2,1)S(1)} %get-tuple-element.9.up, bf16[2048,1024]{1,0:T(8,128)(2,1)S(1)} %get-tuple-element.10.down, ...), custom_call_target="tpu_custom_call" | custom-call | tf_op jit(solution)/shard_map/pallas_call | solution.py:687
  (2 shorter events, 0.0 us)
Async XLA Ops:
  0.6 0.7 copy-start
  2.2 1.4 copy-start.1
  3.6 0.7 copy-start.2
